TPU v7x, 256 devices: a whole 4x4x8 slice. The times are simulated.
256 devices in a mesh: sp: 64 (over z, x, core), tp: 4 (over y).
Axes of the slice: x: 4, y: 4, z: 8, core: 2. Of those that a mesh axis runs over, the one named last changes fastest.
Arguments:
- mid: bfloat16 [12288, 2048], P('sp'), may hold values from -6 to 6
- out_grad: bfloat16 [12288, 2048], P('sp'), may hold values from -16 to 16
- expert_ids: int32 [12288, 2], P('sp'), may hold values from 0 to 63, all different within a row; in each aligned block of 192 rows (0 to 191, 192 to 383, ...) at most 9 rows name the same one
- route_weights: float32 [12288, 2], P('sp'), may hold values from 0.1 to 0.9
- gate_proj: bfloat16 [64, 2048, 1024], P('sp', None, 'tp'), may hold values from -0.375 to 0.375
- up_proj: bfloat16 [64, 2048, 1024], P('sp', None, 'tp'), may hold values from -0.375 to 0.375
- down_proj: bfloat16 [64, 1024, 2048], P('sp', 'tp'), may hold values from -0.1875 to 0.1875
- out_proj: bfloat16 [512, 2048], P('tp'), may hold values from -0.25 to 0.25
- branch_gate: bfloat16 [12288, 512], P('sp', 'tp'), may hold values from -6 to 6
- conv_out: bfloat16 [2, 12288, 512], P(None, 'sp', 'tp'), may hold values from -6 to 6
- prior_state: float32 [2, 12288, 512], P(None, 'sp', 'tp'), may hold values from -6 to 6
- rate_gate_w: bfloat16 [2, 8, 64, 64], P(None, 'tp'), may hold values from -0.75 to 0.75
- input_gate_w: bfloat16 [2, 8, 64, 64], P(None, 'tp'), may hold values from -0.75 to 0.75
- decay_param: float32 [2, 512], P(None, 'tp'), may hold values from 4 to 16
- decay_jump: float32 [2, 12288, 512], P(None, 'sp', 'tp'), may hold values from -2 to 0
- conv_taps: bfloat16 [2, 4, 512], P(None, None, 'tp'), may hold values from -3 to 3
Outputs:
- gate_grad: bfloat16 [64, 2048, 1024], P('sp', None, 'tp')
- up_grad: bfloat16 [64, 2048, 1024], P('sp', None, 'tp')
- down_grad: bfloat16 [64, 1024, 2048], P('sp', 'tp')
- proj_grad_t: float32 [2048, 512], P('sp', 'tp')
- input_grad: bfloat16 [12288, 512], P('sp', 'tp')
- branch_gate_grad: bfloat16 [12288, 512], P('sp', 'tp')
Inputs may be any that keep to these rules, and one draw needn't show every extreme that they name: `expert_ids`: each row names 2 different experts. Among the rows of one device no expert is named by more than 9 rows, a bound that some block reaches of some device.
All inputs are finite; a program needn't handle non-finite values.
Results may differ from a plain program's by a relative error of at most 0.023.
The roundings to bfloat16 on the way count: a program that leaves them out, or rounds other values in their place, can miss the bound.
Values may be sent and summed in bfloat16 or wider, within the bound.
No kernel may reach another device: no remote copies, remote signals or barrier semaphores. Data moves between devices by JAX's collectives and lax.ppermute only.
A program may use at most 64 MiB of HBM per device.

v0:
```python
import jax
import jax.numpy as jnp
from jax import lax
from jax.experimental import pallas as pl
from jax.experimental.pallas import tpu as pltpu
from jax.sharding import PartitionSpec as P

RATE_SCALE = 8.0
CLAMP_LIMIT = 7.0
SHARPNESS = 1.702
NORM_EPSILON = 1e-06
STATE_FLOOR = 0.001
GELU_CUBIC = 0.044715
GELU_SCALE = 0.7978845608028654
LANES = 128


def ring_pairs(axis):
    count = lax.axis_size(axis)
    forward = [(i, (i + 1) % count) for i in range(count)]
    return forward, [(target, source) for source, target in forward]


def ring_blocks(x, axis):
    forward, backward = ring_pairs(axis)
    half = x.shape[0] // 2
    left = lax.ppermute(x, axis, forward)
    right = lax.ppermute(x, axis, backward)
    left_cut, right_cut = left[:half], right[half:]
    far_top = lax.ppermute(left_cut, axis, forward)
    far_bottom = lax.ppermute(right_cut, axis, backward)
    return x, right, far_top, far_bottom, left


def gelu_parts(values):
    inside = GELU_SCALE * (values + GELU_CUBIC * values * values * values)
    tangent = jnp.tanh(inside)
    result = 0.5 * values * (1.0 + tangent)
    slope_value = 0.5 * (1.0 + tangent) + 0.5 * values * (1.0 - tangent * tangent) * GELU_SCALE * (
        1.0 + 3.0 * GELU_CUBIC * values * values
    )
    return (result, slope_value)


SEGMENTS = 8
EDGE = 8


def over_segments(a_rows, b_rows, order):
    carry, factor = jnp.zeros_like(a_rows[:1]), jnp.ones_like(a_rows[:1])
    carries, factors = [None] * SEGMENTS, [None] * SEGMENTS
    for s in order:
        carries[s], factors[s] = carry, factor
        a, b = a_rows[s : s + 1], b_rows[s : s + 1]
        carry, factor = a * carry + b, a * factor
    return jnp.concatenate(carries), jnp.concatenate(factors), factor, carry


def scan_side(seed_ref, decay_ref, local_ref, prod_ref, base, rows, reverse):
    step = rows // SEGMENTS

    def at(i):
        return pl.ds(base + i, SEGMENTS, stride=step)

    order = list(range(step))[::-1] if reverse else list(range(step))
    value = factor = last = None
    for i in order:
        seed = seed_ref[pl.ds(i, SEGMENTS, stride=step), :]
        value = seed if value is None else seed + last * value
        factor = jnp.ones_like(seed) if factor is None else factor * last
        local_ref[at(i), :] = value
        prod_ref[at(i), :] = factor
        last = decay_ref[at(i), :]
    segs = range(SEGMENTS)[::-1] if reverse else range(SEGMENTS)
    carries, factors, whole_factor, whole_value = over_segments(
        factor * last, value * last, segs
    )
    for i in range(step):
        prod = prod_ref[at(i), :]
        local_ref[at(i), :] = local_ref[at(i), :] + prod * carries
        prod_ref[at(i), :] = prod * factors
    return whole_factor, whole_value


def branch_kernel(
    token_ref,
    mid_ref,
    inv_ref,
    cot_ref,
    out_proj_ref,
    states_ref,
    gelu_ref,
    slope_ref,
    decay_ref,
    mixed_ref,
    first_ref,
    last_ref,
    gate_out_ref,
    local_ref,
    prod_ref,
    send_ref,
    low_ref,
    high_ref,
    seed_ref,
):
    shards = send_ref.shape[0]
    share = shards // token_ref.shape[0]
    piece = token_ref.shape[2] // share
    groups, rows, span = token_ref.shape
    inv = inv_ref[...]
    total = jnp.zeros_like(inv)
    for k in range(groups):
        cols = slice(k * span, (k + 1) * span)
        normed = mid_ref[:, cols].astype(jnp.float32) * inv
        total = total + jnp.sum(
            token_ref[k].astype(jnp.float32) * normed, axis=1, keepdims=True
        )
    mean = total / (groups * span)
    branch = jnp.zeros(states_ref.shape, jnp.float32)
    for k in range(groups):
        cols = slice(k * span, (k + 1) * span)
        normed = mid_ref[:, cols].astype(jnp.float32) * inv
        grad = (
            cot_ref[:, cols].astype(jnp.float32)
            + inv * (token_ref[k].astype(jnp.float32) - normed * mean)
        ).astype(jnp.bfloat16)
        branch = branch + last_dims(grad, out_proj_ref[:, cols])
        proj = first_dims(grad, mixed_ref[...]).astype(jnp.bfloat16)
        send_ref[k * share : (k + 1) * share, :piece, :] = proj.reshape(share, piece, LANES)
    gate_out_ref[...] = (branch * states_ref[...] * slope_ref[...]).astype(jnp.bfloat16)
    seed_ref[...] = branch * gelu_ref[...]
    later = scan_side(seed_ref, decay_ref, local_ref, prod_ref, 0, rows, True)
    earlier = scan_side(seed_ref, decay_ref, local_ref, prod_ref, rows, rows, False)
    maps = jnp.concatenate([*later, *earlier])
    high_part = maps.astype(jnp.bfloat16)
    low_part = (maps - high_part.astype(jnp.float32)).astype(jnp.bfloat16)
    pair = jnp.concatenate(
        [high_part.astype(jnp.float32), low_part.astype(jnp.float32)]
    ).astype(jnp.bfloat16)
    send_ref[:, piece:, :] = jnp.broadcast_to(pair[None], (shards, *pair.shape))
    low_ref[:EDGE] = local_ref[:EDGE]
    low_ref[EDGE : 2 * EDGE] = prod_ref[:EDGE]
    low_ref[2 * EDGE :] = first_ref[...]
    high_ref[:EDGE] = local_ref[2 * rows - EDGE :]
    high_ref[EDGE : 2 * EDGE] = prod_ref[2 * rows - EDGE :]
    high_ref[2 * EDGE :] = last_ref[...]


def folded(maps_ref, which, kept, reverse):
    count = maps_ref.shape[0] // 8
    step = count // SEGMENTS
    lead = step * lax.broadcasted_iota(jnp.int32, (SEGMENTS, LANES), 0)
    value = jnp.zeros((SEGMENTS, LANES), jnp.float32)
    factor = jnp.ones((SEGMENTS, LANES), jnp.float32)
    for i in range(step)[::-1] if reverse else range(step):
        use = kept(lead + i)
        a, b = (
            maps_ref[pl.ds(8 * i + q, SEGMENTS, stride=8 * step), :]
            + maps_ref[pl.ds(8 * i + q + 4, SEGMENTS, stride=8 * step), :]
            for q in (which, which + 1)
        )
        a, b = jnp.where(use, a, 1.0), jnp.where(use, b, 0.0)
        value, factor = a * value + b, factor * a
    carry = jnp.zeros((1, LANES), jnp.float32)
    for s in range(SEGMENTS)[::-1] if reverse else range(SEGMENTS):
        carry = factor[s : s + 1] * carry + value[s : s + 1]
    return carry


def tail_kernel(
    here_ref,
    got_ref,
    local_ref,
    prod_ref,
    drive_ref,
    rate_ref,
    input_ref,
    after_ref,
    before_ref,
    rate_w_ref,
    input_w_ref,
    taps_ref,
    out_ref,
    proj_ref,
    later_ref,
    earlier_ref,
    maps_ref,
):
    here = here_ref[0]
    piece = proj_ref.shape[0]
    proj_ref[...] = jnp.sum(got_ref[:, :piece, :].astype(jnp.float32), axis=0)
    maps_ref[...] = got_ref[:, piece:, :].astype(jnp.float32).reshape(maps_ref.shape)
    rows = out_ref.shape[0]
    reach = taps_ref.shape[0] // 2 - 1

    def spread(side, adjoint, drive, rate, inp):
        def back(coef, w_ref):
            return lax.dot_general(
                (adjoint * coef).astype(jnp.bfloat16),
                w_ref[side],
                (((1,), (1,)), ((), ())),
                preferred_element_type=jnp.float32,
            )

        return adjoint * drive + back(rate, rate_w_ref) + back(inp, input_w_ref)

    def main(side, inflow):
        own = slice(side * rows, (side + 1) * rows)
        adjoint = local_ref[own] + prod_ref[own] * inflow
        return spread(side, adjoint, drive_ref[own], rate_ref[own], input_ref[own])

    def edge(side, ref, inflow):
        part = [ref[k * EDGE : (k + 1) * EDGE] for k in range(5)]
        return spread(side, part[0] + part[1] * inflow, *part[2:])

    later_ref[:rows] = main(0, folded(maps_ref, 0, lambda j: j > here, True))
    later_ref[rows:] = edge(0, after_ref, folded(maps_ref, 0, lambda j: j > here + 1, True))
    earlier_ref[:EDGE] = edge(
        1, before_ref, folded(maps_ref, 2, lambda j: j < here - 1, False)
    )
    earlier_ref[EDGE:] = main(1, folded(maps_ref, 2, lambda j: j < here, False))
    total = jnp.zeros((rows, LANES), jnp.float32)
    for k in range(reach + 1):
        up, down = reach - k, EDGE - reach + k
        total = total + taps_ref[k : k + 1] * later_ref[up : up + rows]
        total = (
            total
            + taps_ref[reach + 1 + k : reach + 2 + k] * earlier_ref[down : down + rows]
        )
    out_ref[...] = total.astype(jnp.bfloat16)


ROOM_PAD = 40
VMEM_ROOM = 24 << 20


def row_of(slot, part, parts):
    return slot * parts + part


def pack_rows(value, scratch_ref, out_ref, room):
    shards = out_ref.shape[0]
    parts = value.shape[1] // LANES
    for r in range(room):
        for c in range(parts):
            scratch_ref[pl.ds(row_of(r, c, parts), shards, stride=ROOM_PAD), :] = value[
                r * shards : (r + 1) * shards, c * LANES : (c + 1) * LANES
            ]
    for extra in range(room * parts, ROOM_PAD):
        scratch_ref[pl.ds(extra, shards, stride=ROOM_PAD), :] = jnp.zeros(
            (shards, LANES), jnp.float32
        )
    out_ref[...] = scratch_ref[...].reshape(out_ref.shape).astype(jnp.bfloat16)


def unpack_rows(in_ref, scratch_ref, out_ref, room):
    shards = in_ref.shape[0]
    parts = out_ref.shape[1] // LANES
    scratch_ref[...] = in_ref[...].astype(jnp.float32).reshape(scratch_ref.shape)
    for r in range(room):
        for c in range(parts):
            out_ref[r * shards : (r + 1) * shards, c * LANES : (c + 1) * LANES] = scratch_ref[
                pl.ds(row_of(r, c, parts), shards, stride=ROOM_PAD), :
            ].astype(jnp.bfloat16)


def first_dims(a, b):
    return lax.dot_general(a, b, (((0,), (0,)), ((), ())), preferred_element_type=jnp.float32)


def last_dims(a, b):
    return lax.dot_general(a, b, (((1,), (1,)), ((), ())), preferred_element_type=jnp.float32)


def plain(a, b):
    return jnp.dot(a, b, preferred_element_type=jnp.float32)


def route_kernel(
    place_ref, ids_ref, mid_ref, packed_ref, inv_ref, pick0_ref, pick1_ref, scratch_ref
):
    rows, width = mid_ref.shape
    shards = packed_ref.shape[0]
    slots = pick0_ref.shape[0]
    span = packed_ref.shape[1] * LANES // (slots // shards) // LANES * LANES
    ids = ids_ref[...]
    experts = lax.broadcasted_iota(jnp.int32, (shards, rows), 0)
    hits = [ids[k : k + 1] == experts for k in range(2)]
    named = (hits[0] | hits[1]).astype(jnp.bfloat16)
    earlier = (
        lax.broadcasted_iota(jnp.int32, (rows, rows), 0)
        < lax.broadcasted_iota(jnp.int32, (rows, rows), 1)
    ).astype(jnp.bfloat16)
    ranks = plain(named, earlier)
    tall = lax.broadcasted_iota(jnp.int32, (slots, rows), 0)
    picks = []
    for k, ref in enumerate((pick0_ref, pick1_ref)):
        rank = jnp.sum(jnp.where(hits[k], ranks, 0.0), axis=0, keepdims=True)
        target = rank.astype(jnp.int32) * shards + ids[k : k + 1]
        pick = (tall == target).astype(jnp.bfloat16)
        ref[...] = pick
        picks.append(pick)
    total = jnp.zeros((rows, 1), jnp.float32)
    step = 512
    for c in range(width // step):
        part = mid_ref[:, c * step : (c + 1) * step].astype(jnp.float32)
        total = total + jnp.sum(part * part, axis=1, keepdims=True)
    inv = lax.rsqrt(total / width + NORM_EPSILON)
    inv_ref[...] = inv
    own = mid_ref[:, pl.ds(pl.multiple_of(place_ref[0] * span, LANES), span)]
    normed = (own.astype(jnp.float32) * inv).astype(jnp.bfloat16)
    pack_rows(plain(picks[0] + picks[1], normed), scratch_ref, packed_ref, slots // shards)


def weigh_kernel(place_ref, weights_ref, cot_ref, pick0_ref, pick1_ref, packed_ref, scratch_ref):
    shards = packed_ref.shape[0]
    slots = pick0_ref.shape[0]
    span = packed_ref.shape[1] * LANES // (slots // shards) // LANES * LANES
    own = cot_ref[:, pl.ds(pl.multiple_of(place_ref[0] * span, LANES), span)]
    weight = jnp.sum(
        pick0_ref[...].astype(jnp.float32) * weights_ref[0:1]
        + pick1_ref[...].astype(jnp.float32) * weights_ref[1:2],
        axis=1,
        keepdims=True,
    )
    total = plain(pick0_ref[...] + pick1_ref[...], own) * weight
    pack_rows(total, scratch_ref, packed_ref, slots // shards)


def unpack_kernel(in_ref, out_ref, scratch_ref):
    unpack_rows(in_ref, scratch_ref, out_ref, out_ref.shape[0] // in_ref.shape[0])


def offsets(place_ref, groups, span):
    return [
        pl.multiple_of(lax.rem(place_ref[0] + k, groups) * span, span) for k in range(groups)
    ]


def forward_kernel(
    place_ref,
    own_ref,
    right_ref,
    top_ref,
    bottom_ref,
    left_ref,
    gate_ref,
    up_ref,
    act_ref,
    gate_factor_ref,
    up_factor_ref,
):
    _, span = top_ref.shape
    at = offsets(place_ref, gate_ref.shape[0] // span, span)
    far = jnp.concatenate([top_ref[...], bottom_ref[...]])

    def pre(w_ref):
        total = plain(own_ref[...], w_ref[pl.ds(at[0], span), :])
        total = total + plain(right_ref[...], w_ref[pl.ds(at[1], span), :])
        total = total + plain(left_ref[...], w_ref[pl.ds(at[3], span), :])
        return total + plain(far, w_ref[pl.ds(at[2], span), :])

    gate_pre = pre(gate_ref)
    up_pre = pre(up_ref)
    gate = jnp.minimum(gate_pre, CLAMP_LIMIT)
    up_one = jnp.clip(up_pre, -CLAMP_LIMIT, CLAMP_LIMIT) + 1.0
    sig = jax.nn.sigmoid(SHARPNESS * gate)
    swish = gate * sig
    act_ref[...] = (up_one * swish).astype(jnp.bfloat16)
    gate_factor_ref[...] = jnp.where(
        gate_pre < CLAMP_LIMIT, up_one * (sig + SHARPNESS * swish * (1.0 - sig)), 0.0
    )
    up_factor_ref[...] = jnp.where(jnp.abs(up_pre) < CLAMP_LIMIT, swish, 0.0)


def near_kernel(place_ref, own_ref, right_ref, left_ref, down_ref, total_ref):
    span = own_ref.shape[1]
    at = offsets(place_ref, down_ref.shape[1] // span, span)
    total = last_dims(own_ref[...], down_ref[:, pl.ds(at[0], span)])
    total = total + last_dims(right_ref[...], down_ref[:, pl.ds(at[1], span)])
    total_ref[...] = total + last_dims(left_ref[...], down_ref[:, pl.ds(at[3], span)])


def delta_kernel(
    place_ref,
    near_ref,
    top_ref,
    bottom_ref,
    down_ref,
    gate_ref,
    up_ref,
    gate_factor_ref,
    up_factor_ref,
    gate_delta_ref,
    up_delta_ref,
    far_top_ref,
    far_bottom_ref,
):
    half, span = top_ref.shape
    at = offsets(place_ref, gate_ref.shape[0] // span, span)
    far = jnp.concatenate([top_ref[...], bottom_ref[...]])
    act_grad = near_ref[...] + last_dims(far, down_ref[:, pl.ds(at[2], span)])
    gate_delta = (act_grad * gate_factor_ref[...]).astype(jnp.bfloat16)
    up_delta = (act_grad * up_factor_ref[...]).astype(jnp.bfloat16)
    gate_delta_ref[...] = gate_delta
    up_delta_ref[...] = up_delta
    out = (
        last_dims(gate_delta, gate_ref[pl.ds(at[2], span), :])
        + last_dims(up_delta, up_ref[pl.ds(at[2], span), :])
    ).astype(jnp.bfloat16)
    far_top_ref[...] = out[:half]
    far_bottom_ref[...] = out[half:]


def partial_kernel(place_ref, gate_delta_ref, up_delta_ref, gate_ref, up_ref, *out_refs):
    span = out_refs[0].shape[1]
    at = offsets(place_ref, gate_ref.shape[0] // span, span)
    for k, ref in zip((1, 3, 0), out_refs):
        ref[...] = last_dims(gate_delta_ref[...], gate_ref[pl.ds(at[k], span), :]) + last_dims(
            up_delta_ref[...], up_ref[pl.ds(at[k], span), :]
        )


def relay_kernel(right_ref, left_ref, from_left_ref, from_right_ref, to_right_ref, to_left_ref):
    half = from_left_ref.shape[0]
    bf = jnp.bfloat16
    to_right_ref[:half] = (right_ref[:half] + from_left_ref[...].astype(jnp.float32)).astype(bf)
    to_right_ref[half:] = right_ref[half:].astype(bf)
    to_left_ref[:half] = left_ref[:half].astype(bf)
    to_left_ref[half:] = (left_ref[half:] + from_right_ref[...].astype(jnp.float32)).astype(bf)


def gather_kernel(own_ref, from_left_ref, from_right_ref, packed_ref, scratch_ref):
    total = (
        own_ref[...]
        + from_left_ref[...].astype(jnp.float32)
        + from_right_ref[...].astype(jnp.float32)
    )
    pack_rows(total, scratch_ref, packed_ref, total.shape[0] // packed_ref.shape[0])


def combine_kernel(in_ref, pick0_ref, pick1_ref, out_ref, scratch_ref, rows_ref):
    unpack_rows(in_ref, scratch_ref, rows_ref, rows_ref.shape[0] // in_ref.shape[0])
    total = first_dims(pick0_ref[...] + pick1_ref[...], rows_ref[...]).astype(jnp.bfloat16)
    for k in range(out_ref.shape[0]):
        out_ref[k] = total


def weights_kernel(
    place_ref,
    r_own_ref,
    r_right_ref,
    r_top_ref,
    r_bottom_ref,
    r_left_ref,
    g_own_ref,
    g_right_ref,
    g_top_ref,
    g_bottom_ref,
    g_left_ref,
    act_ref,
    gate_delta_ref,
    up_delta_ref,
    gate_out_ref,
    up_out_ref,
    down_out_ref,
):
    _, span = r_top_ref.shape
    at = offsets(place_ref, gate_out_ref.shape[0] // span, span)
    rows = (r_own_ref, r_right_ref, (r_top_ref, r_bottom_ref), r_left_ref)
    grads = (g_own_ref, g_right_ref, (g_top_ref, g_bottom_ref), g_left_ref)
    bf = jnp.bfloat16

    def whole(block):
        if isinstance(block, tuple):
            return jnp.concatenate([part[...] for part in block])
        return block[...]

    for k in range(4):
        row = whole(rows[k])
        gate_out_ref[pl.ds(at[k], span), :] = first_dims(row, gate_delta_ref[...]).astype(bf)
        up_out_ref[pl.ds(at[k], span), :] = first_dims(row, up_delta_ref[...]).astype(bf)
        down_out_ref[:, pl.ds(at[k], span)] = first_dims(act_ref[...], whole(grads[k])).astype(bf)


def on_device(
    mid,
    out_grad,
    expert_ids,
    route_weights,
    gate_proj,
    up_proj,
    down_proj,
    out_proj,
    branch_gate,
    conv_out,
    prior_state,
    rate_gate_w,
    input_gate_w,
    decay_param,
    decay_jump,
    conv_taps,
):
    tok_rows, embedding_width = mid.shape
    shards = lax.axis_size("sp")
    groups = lax.axis_size("tp")
    local_experts = gate_proj.shape[0]
    experts_all = local_experts * shards
    top_count = expert_ids.shape[1]
    expert_room = 3 * top_count * tok_rows // (2 * experts_all)
    slot_count = experts_all * expert_room
    span = embedding_width // groups
    hidden = gate_proj.shape[2]
    bf16, f32 = (jnp.bfloat16, jnp.float32)

    def shaped(*dims, dtype=bf16):
        return jax.ShapeDtypeStruct(dims, dtype)

    vmem = pl.BlockSpec(memory_space=pltpu.VMEM)
    smem = pl.BlockSpec(memory_space=pltpu.SMEM)

    def kernel(body, outs, *args, scalar=None, scratch=(), flops=0):
        lead = () if scalar is None else (scalar,)
        return pl.pallas_call(
            body,
            out_shape=outs,
            in_specs=[smem] * len(lead) + [vmem] * len(args),
            scratch_shapes=list(scratch),
            compiler_params=pltpu.CompilerParams(vmem_limit_bytes=VMEM_ROOM),
            cost_estimate=pl.CostEstimate(flops=flops, transcendentals=0, bytes_accessed=0),
        )(*lead, *args)

    packed_shape = shaped(shards, ROOM_PAD, LANES)
    pack_scratch = pltpu.VMEM((shards * ROOM_PAD, LANES), f32)
    place = lax.axis_index("tp").astype(jnp.int32).reshape(1)
    pick_shape = shaped(slot_count, tok_rows)
    sent_rows, inv_rms, pick0, pick1 = kernel(
        route_kernel,
        (packed_shape, shaped(tok_rows, 1, dtype=f32), pick_shape, pick_shape),
        expert_ids.T,
        mid,
        scalar=place,
        scratch=(pack_scratch,),
    )
    sent_grad = kernel(
        weigh_kernel,
        packed_shape,
        route_weights.T,
        out_grad,
        pick0,
        pick1,
        scalar=place,
        scratch=(pack_scratch,),
        flops=1 << 28,
    )
    heads_local = rate_gate_w.shape[1]
    head_width = rate_gate_w.shape[2]
    channels = heads_local * head_width

    def on_diagonal(w):
        return jnp.concatenate(
            [
                jnp.pad(
                    w[:, h],
                    ((0, 0), (0, 0), (h * head_width, channels - (h + 1) * head_width)),
                )
                for h in range(heads_local)
            ],
            axis=1,
        )

    rate_blocks, input_blocks = on_diagonal(rate_gate_w), on_diagonal(input_gate_w)

    def gate_of(blocks):
        return jax.nn.sigmoid(
            jnp.einsum("stc,scd->std", conv_out, blocks, preferred_element_type=jnp.float32)
        )

    rate_gate, input_gate = gate_of(rate_blocks), gate_of(input_blocks)
    decay_rate = jax.nn.softplus(-decay_param)[:, None, :]
    log_decay = -RATE_SCALE * rate_gate * decay_rate + decay_jump
    decay_factors = jnp.exp(log_decay)
    squared = jnp.exp(2.0 * log_decay)
    norm_factor = jnp.sqrt(STATE_FLOOR - jnp.expm1(2.0 * log_decay))
    conv_full = conv_out.astype(jnp.float32)
    drive_term = input_gate * conv_full
    decayed = decay_factors * prior_state
    states = decayed + norm_factor * drive_term
    summed_states = states[0] + states[1]
    gelu_value, gelu_slope = gelu_parts(branch_gate.astype(jnp.float32))
    mixed_b = (summed_states * gelu_value).astype(jnp.bfloat16)
    rate_coef = (
        (decayed - drive_term * squared / norm_factor)
        * (-RATE_SCALE * decay_rate)
        * rate_gate
        * (1.0 - rate_gate)
    )
    drive_coef = norm_factor * input_gate
    input_coef = norm_factor * conv_full * input_gate * (1.0 - input_gate)
    first_edge = jnp.concatenate([c[0, :EDGE] for c in (drive_coef, rate_coef, input_coef)])
    last_edge = jnp.concatenate([c[1, -EDGE:] for c in (drive_coef, rate_coef, input_coef)])
    (
        sent_grad,
        decay_factors,
        summed_states,
        gelu_value,
        gelu_slope,
        mixed_b,
        rate_coef,
        drive_coef,
        input_coef,
        first_edge,
        last_edge,
    ) = lax.optimization_barrier(
        (
            sent_grad,
            decay_factors,
            summed_states,
            gelu_value,
            gelu_slope,
            mixed_b,
            rate_coef,
            drive_coef,
            input_coef,
            first_edge,
            last_edge,
        )
    )

    def unpacked(x):
        return kernel(unpack_kernel, shaped(slot_count, span), x, scratch=(pack_scratch,))

    got_rows = lax.all_to_all(sent_rows, "sp", 0, 0, tiled=True)
    rows = ring_blocks(unpacked(got_rows), "tp")
    got_grad = lax.all_to_all(sent_grad, "sp", 0, 0, tiled=True)
    grads = ring_blocks(unpacked(got_grad), "tp")
    wide_hidden = shaped(slot_count, hidden, dtype=f32)
    act, gate_factor, up_factor = kernel(
        forward_kernel,
        (shaped(slot_count, hidden), wide_hidden, wide_hidden),
        *rows,
        gate_proj[0],
        up_proj[0],
        scalar=place,
        flops=1 << 31,
    )
    half = slot_count // 2
    forward, backward = ring_pairs("tp")
    near = kernel(
        near_kernel,
        wide_hidden,
        grads[0],
        grads[1],
        grads[4],
        down_proj[0],
        scalar=place,
        flops=1 << 30,
    )
    gate_delta, up_delta, far_top, far_bottom = kernel(
        delta_kernel,
        (
            shaped(slot_count, hidden),
            shaped(slot_count, hidden),
            shaped(half, span),
            shaped(half, span),
        ),
        near,
        grads[2],
        grads[3],
        down_proj[0],
        gate_proj[0],
        up_proj[0],
        gate_factor,
        up_factor,
        scalar=place,
    )
    from_left = lax.ppermute(far_top, "tp", forward)
    from_right = lax.ppermute(far_bottom, "tp", backward)
    part = shaped(slot_count, span, dtype=f32)
    for_right, for_left, for_own = kernel(
        partial_kernel,
        (part, part, part),
        gate_delta,
        up_delta,
        gate_proj[0],
        up_proj[0],
        scalar=place,
        flops=1 << 30,
    )
    to_right, to_left = kernel(
        relay_kernel,
        (shaped(slot_count, span), shaped(slot_count, span)),
        for_right,
        for_left,
        from_left,
        from_right,
    )
    got_left = lax.ppermute(to_right, "tp", forward)
    got_right = lax.ppermute(to_left, "tp", backward)
    summed = kernel(
        gather_kernel, packed_shape, for_own, got_left, got_right, scratch=(pack_scratch,)
    )
    returned = lax.all_to_all(summed, "sp", 0, 0, tiled=True)
    token_copies = kernel(
        combine_kernel,
        shaped(groups, tok_rows, span),
        returned,
        pick0,
        pick1,
        scratch=(pack_scratch, pltpu.VMEM((slot_count, span), bf16)),
    )
    token_grad = lax.all_to_all(token_copies, "tp", 0, 0, tiled=True)
    wide = shaped(2 * tok_rows, channels, dtype=f32)
    edges = shaped(5 * EDGE, channels, dtype=f32)
    piece = embedding_width // shards
    branch_gate_grad, local, prod, sent, low, high = kernel(
        branch_kernel,
        (
            shaped(tok_rows, channels),
            wide,
            wide,
            shaped(shards, piece + 8, channels),
            edges,
            edges,
        ),
        token_grad,
        mid,
        inv_rms,
        out_grad,
        out_proj,
        summed_states,
        gelu_value,
        gelu_slope,
        decay_factors.reshape(2 * tok_rows, channels),
        mixed_b,
        first_edge,
        last_edge,
        scratch=(pltpu.VMEM((tok_rows, channels), f32),),
    )
    ring_on = [(i, i + 1) for i in range(shards - 1)]
    ring_back = [(target, source) for source, target in ring_on]
    got = lax.all_to_all(sent, "sp", 0, 0, tiled=True)
    after = lax.ppermute(low, "sp", ring_back)
    before = lax.ppermute(high, "sp", ring_on)
    gate_grad, up_grad, down_grad = kernel(
        weights_kernel,
        (
            shaped(embedding_width, hidden),
            shaped(embedding_width, hidden),
            shaped(hidden, embedding_width),
        ),
        *rows,
        *grads,
        act,
        gate_delta,
        up_delta,
        scalar=place,
        flops=1 << 31,
    )
    here = lax.axis_index("sp").astype(jnp.int32).reshape(1)
    input_grad, proj_grad_t = kernel(
        tail_kernel,
        (shaped(tok_rows, channels), shaped(piece, channels, dtype=f32)),
        got,
        local,
        prod,
        drive_coef.reshape(2 * tok_rows, channels),
        rate_coef.reshape(2 * tok_rows, channels),
        input_coef.reshape(2 * tok_rows, channels),
        after,
        before,
        rate_blocks,
        input_blocks,
        conv_taps.astype(f32).reshape(-1, channels),
        scalar=here,
        scratch=[pltpu.VMEM((tok_rows + EDGE, channels), f32)] * 2
        + [pltpu.VMEM((8 * shards, channels), f32)],
    )
    return (
        gate_grad[None],
        up_grad[None],
        down_grad[None],
        proj_grad_t,
        input_grad,
        branch_gate_grad,
    )


def solution(mesh):
    in_specs = (
        P("sp", None),
        P("sp", None),
        P("sp", None),
        P("sp", None),
        P("sp", None, "tp"),
        P("sp", None, "tp"),
        P("sp", "tp", None),
        P("tp", None),
        P("sp", "tp"),
        P(None, "sp", "tp"),
        P(None, "sp", "tp"),
        P(None, "tp", None, None),
        P(None, "tp", None, None),
        P(None, "tp"),
        P(None, "sp", "tp"),
        P(None, None, "tp"),
    )
    out_specs = (
        P("sp", None, "tp"),
        P("sp", None, "tp"),
        P("sp", "tp", None),
        P("sp", "tp"),
        P("sp", "tp"),
        P("sp", "tp"),
    )

    return jax.shard_map(
        on_device, mesh=mesh, in_specs=in_specs, out_specs=out_specs, check_vma=False
    )
```

profile of v0, /device:TPU:1, one launch (start us, length us, event | category | flops | bytes accessed | tf_op | source)
XLA Modules:
  0.0 193.3 jit_solution(17571747556981178621)
XLA Ops:
  2.5 1.5 shard_map.199
  4.6 13.1 %all-to-all-start = ((bf16[64,40,128]{2,1,0:T(8,128)(2,1)}), bf16[64,40,128]{2,1,0:T(8,128)(2,1)S(1)}, u32[]{:S(2)}, u32[]{:S(2)}) async-start(bf16[64,40,128]{2,1,0:T(8,128)(2,1)} %get-tuple-element.44), calls=%async_computation | async-start | bytes 1310720 | tf_op jit(solution)/shard_map/all_to_all | solution.py:633
  21.8 16.3 %all-to-all-done.in_ref = bf16[64,40,128]{2,1,0:T(8,128)(2,1)S(1)} async-done(((bf16[64,40,128]{2,1,0:T(8,128)(2,1)}), bf16[64,40,128]{2,1,0:T(8,128)(2,1)S(1)}, u32[]{:S(2)}, u32[]{:S(2)}) %all-to-all-start) | async-done | bytes 655392 | tf_op jit(solution)/shard_map/all_to_all | solution.py:633
  38.1 5.8 %all-to-all-start.1 = ((bf16[64,40,128]{2,1,0:T(8,128)(2,1)}), bf16[64,40,128]{2,1,0:T(8,128)(2,1)S(1)}, u32[]{:S(2)}, u32[]{:S(2)}) async-start(bf16[64,40,128]{2,1,0:T(8,128)(2,1)} %shard_map.201), calls=%async_computation.1 | async-start | bytes 1310720 | tf_op jit(solution)/shard_map/all_to_all | solution.py:635
  47.8 16.5 %all-to-all-done.1.in_ref = bf16[64,40,128]{2,1,0:T(8,128)(2,1)S(1)} async-done(((bf16[64,40,128]{2,1,0:T(8,128)(2,1)}), bf16[64,40,128]{2,1,0:T(8,128)(2,1)S(1)}, u32[]{:S(2)}, u32[]{:S(2)}) %all-to-all-start.1) | async-done | bytes 655392 | tf_op jit(solution)/shard_map/all_to_all | solution.py:635
  66.0 1.5 collective-permute-start.4
  69.6 2.7 %collective-permute-start.3 = (bf16[288,512]{1,0:T(8,128)(2,1)S(1)}, bf16[288,512]{1,0:T(8,128)(2,1)S(1)}, u32[]{:S(2)}, u32[]{:S(2)}) collective-permute-start(bf16[288,512]{1,0:T(8,128)(2,1)S(1)} %slice.65), channel_id=1, source_target_pairs={{1,0},{2,1},{3,2},{0,3},{5,4},{6,5},{7,6},{4,7},{9,8},{10,9},{11,1... | collective-permute-start | bytes 884744 | tf_op jit(solution)/shard_map/ppermute | solution.py:31
  72.3 8.0 %collective-permute-done.5.left_ref.g_left_ref = bf16[576,512]{1,0:T(8,128)(2,1)S(1)} collective-permute-done((bf16[576,512]{1,0:T(8,128)(2,1)S(1)}, bf16[576,512]{1,0:T(8,128)(2,1)S(1)}, u32[]{:S(2)}, u32[]{:S(2)}) %collective-permute-start.5) | collective-permute-done | bytes 589856 | tf_op jit(solution)/shard_map/ppermute | solution.py:27
  80.5 2.9 %collective-permute-start.7 = (bf16[288,512]{1,0:T(8,128)(2,1)S(1)}, bf16[288,512]{1,0:T(8,128)(2,1)S(1)}, u32[]{:S(2)}, u32[]{:S(2)}) collective-permute-start(bf16[288,512]{1,0:T(8,128)(2,1)S(1)} %slice.75), channel_id=1, source_target_pairs={{1,0},{2,1},{3,2},{0,3},{5,4},{6,5},{7,6},{4,7},{9,8},{10,9},{11,1... | collective-permute-start | bytes 884744 | tf_op jit(solution)/shard_map/ppermute | solution.py:31
  84.1 2.5 %collective-permute-done.2.top_ref.r_top_ref = bf16[288,512]{1,0:T(8,128)(2,1)S(1)} collective-permute-done((bf16[288,512]{1,0:T(8,128)(2,1)S(1)}, bf16[288,512]{1,0:T(8,128)(2,1)S(1)}, u32[]{:S(2)}, u32[]{:S(2)}) %collective-permute-start.2) | collective-permute-done | bytes 294944 | tf_op jit(solution)/shard_map/ppermute | solution.py:30
  86.7 3.2 %shard_map.203 = (bf16[576,256]{1,0:T(8,128)(2,1)S(1)}, f32[576,256]{1,0:T(8,128)S(1)}, f32[576,256]{1,0:T(8,128)S(1)}) custom-call(s32[1]{0:T(128)} %bitcast.place_ref, bf16[576,512]{1,0:T(8,128)(2,1)} %shard_map.200.own_ref.r_own_ref, bf16[576,512]{1,0:T(8,128)(2,1)} %collective-permute-done.right_ref.r_right_ref, ...), custom_call_target="tpu_custom_call" | custom-call | flops 2147483648 | tf_op jit(solution)/shard_map/pallas_call | solution.py:524
  90.0 3.0 %collective-permute-done.6.top_ref.g_top_ref = bf16[288,512]{1,0:T(8,128)(2,1)S(1)} collective-permute-done((bf16[288,512]{1,0:T(8,128)(2,1)S(1)}, bf16[288,512]{1,0:T(8,128)(2,1)S(1)}, u32[]{:S(2)}, u32[]{:S(2)}) %collective-permute-start.6) | collective-permute-done | bytes 294944 | tf_op jit(solution)/shard_map/ppermute | solution.py:30
  95.0 1.7 collective-permute-start.9
  97.9 4.6 %collective-permute-done.8.from_left_ref = bf16[288,512]{1,0:T(8,128)(2,1)S(1)} collective-permute-done((bf16[288,512]{1,0:T(8,128)(2,1)S(1)}, bf16[288,512]{1,0:T(8,128)(2,1)S(1)}, u32[]{:S(2)}, u32[]{:S(2)}) %collective-permute-start.8) | collective-permute-done | bytes 294944 | tf_op jit(solution)/shard_map/ppermute | solution.py:677
  102.9 2.5 %collective-permute-start.11 = (bf16[576,512]{1,0:T(8,128)(2,1)S(1)}, bf16[576,512]{1,0:T(8,128)(2,1)S(1)}, u32[]{:S(2)}, u32[]{:S(2)}) collective-permute-start(bf16[576,512]{1,0:T(8,128)(2,1)S(1)} %get-tuple-element.62), channel_id=1, source_target_pairs={{1,0},{2,1},{3,2},{0,3},{5,4},{6,5},{7,6},{4,7},{9,8},{10,9},{11,1... | collective-permute-start | bytes 1769480 | tf_op jit(solution)/shard_map/ppermute | solution.py:699
  105.4 11.2 %collective-permute-done.10.from_left_ref = bf16[576,512]{1,0:T(8,128)(2,1)S(1)} collective-permute-done((bf16[576,512]{1,0:T(8,128)(2,1)S(1)}, bf16[576,512]{1,0:T(8,128)(2,1)S(1)}, u32[]{:S(2)}, u32[]{:S(2)}) %collective-permute-start.10) | collective-permute-done | bytes 589856 | tf_op jit(solution)/shard_map/ppermute | solution.py:698
  117.1 29.3 %all_to_all.25.in_ref = bf16[64,40,128]{2,1,0:T(8,128)(2,1)S(1)} all-to-all(bf16[64,40,128]{2,1,0:T(8,128)(2,1)S(1)} %shard_map.209), channel_id=1, replica_groups=mesh['sp'=64,'tp'=4] {'sp'}, dimensions={0} | all-to-all | bytes 1310720 | tf_op jit(solution)/shard_map/all_to_all | solution.py:703
  147.1 15.2 %all_to_all.26.token_ref = bf16[4,192,512]{2,1,0:T(8,128)(2,1)S(1)} all-to-all(bf16[4,192,512]{2,1,0:T(8,128)(2,1)S(1)} %shard_map.210), channel_id=1, replica_groups=mesh['sp'=64,'tp'=4] {'tp'}, dimensions={0} | all-to-all | bytes 1572864 | tf_op jit(solution)/shard_map/all_to_all | solution.py:712
  162.3 2.3 %shard_map.211 = (bf16[192,128]{1,0:T(8,128)(2,1)}, f32[384,128]{1,0:T(8,128)S(1)}, f32[384,128]{1,0:T(8,128)S(1)}, bf16[64,40,128]{2,1,0:T(8,128)(2,1)}, f32[40,128]{1,0:T(8,128)S(1)}, /*index=5*/f32[40,128]{1,0:T(8,128)S(1)}) custom-call(bf16[4,192,512]{2,1,0:T(8,128)(2,1)S(1)} %all_to_all.26.token_ref, bf16[192,2048]{1,0:T(8,128)(2,1)S(1)} %copy-done.1, ...), custom_call_target="tpu_custom_call" | custom-call | tf_op jit(solution)/shard_map/pallas_call | solution.py:524
  164.7 7.1 %all-to-all-start.4 = ((bf16[64,40,128]{2,1,0:T(8,128)(2,1)}), bf16[64,40,128]{2,1,0:T(8,128)(2,1)S(1)}, u32[]{:S(2)}, u32[]{:S(2)}) async-start(bf16[64,40,128]{2,1,0:T(8,128)(2,1)} %get-tuple-element.71), calls=%async_computation.4 | async-start | bytes 1310720 | tf_op jit(solution)/shard_map/all_to_all | solution.py:742
  171.9 2.4 %collective-permute-start.12 = (f32[40,128]{1,0:T(8,128)S(1)}, f32[40,128]{1,0:T(8,128)S(1)}, u32[]{:S(2)}, u32[]{:S(2)}) collective-permute-start(f32[40,128]{1,0:T(8,128)S(1)} %get-tuple-element.77), channel_id=1, source_target_pairs={{4,0},{8,4},{12,8},{16,12},{20,16},{24,20},{28,24},{32,28},{36,32}... | collective-permute-start | bytes 61448 | tf_op jit(solution)/shard_map/ppermute | solution.py:743
  174.3 3.4 %collective-permute-start.13 = (f32[40,128]{1,0:T(8,128)S(1)}, f32[40,128]{1,0:T(8,128)S(1)}, u32[]{:S(2)}, u32[]{:S(2)}) collective-permute-start(f32[40,128]{1,0:T(8,128)S(1)} %get-tuple-element.78), channel_id=1, source_target_pairs={{0,4},{4,8},{8,12},{12,16},{16,20},{20,24},{24,28},{28,32},{32,36}... | collective-permute-start | bytes 61448 | tf_op jit(solution)/shard_map/ppermute | solution.py:744
  183.7 5.6 %shard_map.206 = (bf16[2048,256]{1,0:T(8,128)(2,1)}, bf16[2048,256]{1,0:T(8,128)(2,1)}, bf16[256,2048]{1,0:T(8,128)(2,1)}) custom-call(s32[1]{0:T(128)} %bitcast.place_ref, bf16[576,512]{1,0:T(8,128)(2,1)} %shard_map.200.own_ref.r_own_ref, bf16[576,512]{1,0:T(8,128)(2,1)} %collective-permute-done.right_ref.r_right_ref, bf16[288,512]{1,0:T(8,128)(2,1)S(1)} %copy-done.25, ...), custom_call_target="tpu_custom_call" | custom-call | flops 2147483648 | tf_op jit(solution)/shard_map/pallas_call | solution.py:524
  189.3 2.8 %all-to-all-done.4.got_ref = bf16[64,40,128]{2,1,0:T(8,128)(2,1)S(1)} async-done(((bf16[64,40,128]{2,1,0:T(8,128)(2,1)}), bf16[64,40,128]{2,1,0:T(8,128)(2,1)S(1)}, u32[]{:S(2)}, u32[]{:S(2)}) %all-to-all-start.4) | async-done | bytes 655392 | tf_op jit(solution)/shard_map/all_to_all | solution.py:742
  (143 shorter events, 26.6 us)
Async XLA Ops:
  0.6 17.1 %copy-start.48 = (f32[2,128]{1,0:T(2,128)S(1)}, f32[2,128]{1,0:T(2,128)}, u32[]{:S(2)}) copy-start(f32[2,128]{1,0:T(2,128)} %param.29) | copy-start | bytes 3076
  2.5 15.3 %copy-start.44 = (bf16[2,2,64,64]{3,2,1,0:T(8,128)(2,1)S(1)}, bf16[2,2,64,64]{3,2,1,0:T(8,128)(2,1)}, u32[]{:S(2)}) copy-start(bf16[2,2,64,64]{3,2,1,0:T(8,128)(2,1)} %param.27) | copy-start | bytes 98308
  2.5 15.4 %copy-start.45 = (bf16[2,2,64,64]{3,2,1,0:T(8,128)(2,1)S(1)}, bf16[2,2,64,64]{3,2,1,0:T(8,128)(2,1)}, u32[]{:S(2)}) copy-start(bf16[2,2,64,64]{3,2,1,0:T(8,128)(2,1)} %param.28) | copy-start | bytes 98308
  2.5 15.4 %copy-start.43 = (bf16[2,192,128]{2,1,0:T(8,128)(2,1)S(1)}, bf16[2,192,128]{2,1,0:T(8,128)(2,1)}, u32[]{:S(2)}) copy-start(bf16[2,192,128]{2,1,0:T(8,128)(2,1)} %param.25) | copy-start | bytes 294916
  4.6 33.5 %all-to-all-start = ((bf16[64,40,128]{2,1,0:T(8,128)(2,1)}), bf16[64,40,128]{2,1,0:T(8,128)(2,1)S(1)}, u32[]{:S(2)}, u32[]{:S(2)}) async-start(bf16[64,40,128]{2,1,0:T(8,128)(2,1)} %get-tuple-element.44), calls=%async_computation | async-start | bytes 1310720 | tf_op jit(solution)/shard_map/all_to_all | solution.py:633
  38.1 26.2 %all-to-all-start.1 = ((bf16[64,40,128]{2,1,0:T(8,128)(2,1)}), bf16[64,40,128]{2,1,0:T(8,128)(2,1)S(1)}, u32[]{:S(2)}, u32[]{:S(2)}) async-start(bf16[64,40,128]{2,1,0:T(8,128)(2,1)} %shard_map.201), calls=%async_computation.1 | async-start | bytes 1310720 | tf_op jit(solution)/shard_map/all_to_all | solution.py:635
  45.0 22.5 %collective-permute-start.1 = (bf16[576,512]{1,0:T(8,128)(2,1)}, bf16[576,512]{1,0:T(8,128)(2,1)}, u32[]{:S(2)}, u32[]{:S(2)}) collective-permute-start(bf16[576,512]{1,0:T(8,128)(2,1)} %shard_map.200.own_ref.r_own_ref), channel_id=1, source_target_pairs={{0,1},{1,2},{2,3},{3,0},{4,5},{5,6},{6,7},{7,4},{8,9},{9,10},{10,1... | collective-permute-start | bytes 1769480 | tf_op jit(solution)/shard_map/ppermute | solution.py:27
  46.3 22.2 %collective-permute-start = (bf16[576,512]{1,0:T(8,128)(2,1)}, bf16[576,512]{1,0:T(8,128)(2,1)}, u32[]{:S(2)}, u32[]{:S(2)}) collective-permute-start(bf16[576,512]{1,0:T(8,128)(2,1)} %shard_map.200.own_ref.r_own_ref), channel_id=1, source_target_pairs={{1,0},{2,1},{3,2},{0,3},{5,4},{6,5},{7,6},{4,7},{9,8},{10,9},{11,1... | collective-permute-start | bytes 1769480 | tf_op jit(solution)/shard_map/ppermute | solution.py:28
  64.6 18.9 %copy-start.6 = (bf16[576,512]{1,0:T(8,128)(2,1)}, bf16[576,512]{1,0:T(8,128)(2,1)S(1)}, u32[]{:S(2)}) copy-start(bf16[576,512]{1,0:T(8,128)(2,1)S(1)} %shard_map.202.own_ref.g_own_ref) | copy-start | bytes 1769476
  64.6 18.8 %copy-start.3 = (bf16[1,256,2048]{2,1,0:T(8,128)(2,1)S(1)}, bf16[1,256,2048]{2,1,0:T(8,128)(2,1)}, u32[]{:S(2)}) copy-start(bf16[1,256,2048]{2,1,0:T(8,128)(2,1)} %param.22) | copy-start | bytes 3145732
  64.6 15.8 %collective-permute-start.5 = (bf16[576,512]{1,0:T(8,128)(2,1)S(1)}, bf16[576,512]{1,0:T(8,128)(2,1)S(1)}, u32[]{:S(2)}, u32[]{:S(2)}) collective-permute-start(bf16[576,512]{1,0:T(8,128)(2,1)S(1)} %shard_map.202.own_ref.g_own_ref), channel_id=1, source_target_pairs={{0,1},{1,2},{2,3},{3,0},{4,5},{5,6},{6,7},{7,4},{8,9},{9,10},{10,1... | collective-permute-start | bytes 1769480 | tf_op jit(solution)/shard_map/ppermute | solution.py:27
  66.0 14.5 %collective-permute-start.4 = (bf16[576,512]{1,0:T(8,128)(2,1)S(1)}, bf16[576,512]{1,0:T(8,128)(2,1)S(1)}, u32[]{:S(2)}, u32[]{:S(2)}) collective-permute-start(bf16[576,512]{1,0:T(8,128)(2,1)S(1)} %shard_map.202.own_ref.g_own_ref), channel_id=1, source_target_pairs={{1,0},{2,1},{3,2},{0,3},{5,4},{6,5},{7,6},{4,7},{9,8},{10,9},{11,1... | collective-permute-start | bytes 1769480 | tf_op jit(solution)/shard_map/ppermute | solution.py:28
  68.5 18.2 %collective-permute-start.2 = (bf16[288,512]{1,0:T(8,128)(2,1)S(1)}, bf16[288,512]{1,0:T(8,128)(2,1)S(1)}, u32[]{:S(2)}, u32[]{:S(2)}) collective-permute-start(bf16[288,512]{1,0:T(8,128)(2,1)S(1)} %slice.64), channel_id=1, source_target_pairs={{0,1},{1,2},{2,3},{3,0},{4,5},{5,6},{6,7},{7,4},{8,9},{9,10},{10,1... | collective-permute-start | bytes 884744 | tf_op jit(solution)/shard_map/ppermute | solution.py:30
  69.6 17.1 %collective-permute-start.3 = (bf16[288,512]{1,0:T(8,128)(2,1)S(1)}, bf16[288,512]{1,0:T(8,128)(2,1)S(1)}, u32[]{:S(2)}, u32[]{:S(2)}) collective-permute-start(bf16[288,512]{1,0:T(8,128)(2,1)S(1)} %slice.65), channel_id=1, source_target_pairs={{1,0},{2,1},{3,2},{0,3},{5,4},{6,5},{7,6},{4,7},{9,8},{10,9},{11,1... | collective-permute-start | bytes 884744 | tf_op jit(solution)/shard_map/ppermute | solution.py:31
  80.4 12.6 %collective-permute-start.6 = (bf16[288,512]{1,0:T(8,128)(2,1)S(1)}, bf16[288,512]{1,0:T(8,128)(2,1)S(1)}, u32[]{:S(2)}, u32[]{:S(2)}) collective-permute-start(bf16[288,512]{1,0:T(8,128)(2,1)S(1)} %slice.74), channel_id=1, source_target_pairs={{0,1},{1,2},{2,3},{3,0},{4,5},{5,6},{6,7},{7,4},{8,9},{9,10},{10,1... | collective-permute-start | bytes 884744 | tf_op jit(solution)/shard_map/ppermute | solution.py:30
  80.5 12.5 %collective-permute-start.7 = (bf16[288,512]{1,0:T(8,128)(2,1)S(1)}, bf16[288,512]{1,0:T(8,128)(2,1)S(1)}, u32[]{:S(2)}, u32[]{:S(2)}) collective-permute-start(bf16[288,512]{1,0:T(8,128)(2,1)S(1)} %slice.75), channel_id=1, source_target_pairs={{1,0},{2,1},{3,2},{0,3},{5,4},{6,5},{7,6},{4,7},{9,8},{10,9},{11,1... | collective-permute-start | bytes 884744 | tf_op jit(solution)/shard_map/ppermute | solution.py:31
  94.0 8.5 %collective-permute-start.8 = (bf16[288,512]{1,0:T(8,128)(2,1)S(1)}, bf16[288,512]{1,0:T(8,128)(2,1)S(1)}, u32[]{:S(2)}, u32[]{:S(2)}) collective-permute-start(bf16[288,512]{1,0:T(8,128)(2,1)S(1)} %get-tuple-element.59), channel_id=1, source_target_pairs={{0,1},{1,2},{2,3},{3,0},{4,5},{5,6},{6,7},{7,4},{8,9},{9,10},{10,1... | collective-permute-start | bytes 884744 | tf_op jit(solution)/shard_map/ppermute | solution.py:677
  95.0 7.5 %collective-permute-start.9 = (bf16[288,512]{1,0:T(8,128)(2,1)S(1)}, bf16[288,512]{1,0:T(8,128)(2,1)S(1)}, u32[]{:S(2)}, u32[]{:S(2)}) collective-permute-start(bf16[288,512]{1,0:T(8,128)(2,1)S(1)} %get-tuple-element.60), channel_id=1, source_target_pairs={{1,0},{2,1},{3,2},{0,3},{5,4},{6,5},{7,6},{4,7},{9,8},{10,9},{11,1... | collective-permute-start | bytes 884744 | tf_op jit(solution)/shard_map/ppermute | solution.py:678
  102.7 14.0 %collective-permute-start.10 = (bf16[576,512]{1,0:T(8,128)(2,1)S(1)}, bf16[576,512]{1,0:T(8,128)(2,1)S(1)}, u32[]{:S(2)}, u32[]{:S(2)}) collective-permute-start(bf16[576,512]{1,0:T(8,128)(2,1)S(1)} %get-tuple-element.61), channel_id=1, source_target_pairs={{0,1},{1,2},{2,3},{3,0},{4,5},{5,6},{6,7},{7,4},{8,9},{9,10},{10,1... | collective-permute-start | bytes 1769480 | tf_op jit(solution)/shard_map/ppermute | solution.py:698
  102.9 13.8 %collective-permute-start.11 = (bf16[576,512]{1,0:T(8,128)(2,1)S(1)}, bf16[576,512]{1,0:T(8,128)(2,1)S(1)}, u32[]{:S(2)}, u32[]{:S(2)}) collective-permute-start(bf16[576,512]{1,0:T(8,128)(2,1)S(1)} %get-tuple-element.62), channel_id=1, source_target_pairs={{1,0},{2,1},{3,2},{0,3},{5,4},{6,5},{7,6},{4,7},{9,8},{10,9},{11,1... | collective-permute-start | bytes 1769480 | tf_op jit(solution)/shard_map/ppermute | solution.py:699
  147.0 15.2 %copy-start.1 = (bf16[192,2048]{1,0:T(8,128)(2,1)S(1)}, bf16[192,2048]{1,0:T(8,128)(2,1)}, u32[]{:S(2)}) copy-start(bf16[192,2048]{1,0:T(8,128)(2,1)} %mid_ref.3) | copy-start | bytes 2359300
  164.7 27.4 %all-to-all-start.4 = ((bf16[64,40,128]{2,1,0:T(8,128)(2,1)}), bf16[64,40,128]{2,1,0:T(8,128)(2,1)S(1)}, u32[]{:S(2)}, u32[]{:S(2)}) async-start(bf16[64,40,128]{2,1,0:T(8,128)(2,1)} %get-tuple-element.71), calls=%async_computation.4 | async-start | bytes 1310720 | tf_op jit(solution)/shard_map/all_to_all | solution.py:742
  171.9 17.4 %collective-permute-start.12 = (f32[40,128]{1,0:T(8,128)S(1)}, f32[40,128]{1,0:T(8,128)S(1)}, u32[]{:S(2)}, u32[]{:S(2)}) collective-permute-start(f32[40,128]{1,0:T(8,128)S(1)} %get-tuple-element.77), channel_id=1, source_target_pairs={{4,0},{8,4},{12,8},{16,12},{20,16},{24,20},{28,24},{32,28},{36,32}... | collective-permute-start | bytes 61448 | tf_op jit(solution)/shard_map/ppermute | solution.py:743
  174.3 15.0 %collective-permute-start.13 = (f32[40,128]{1,0:T(8,128)S(1)}, f32[40,128]{1,0:T(8,128)S(1)}, u32[]{:S(2)}, u32[]{:S(2)}) collective-permute-start(f32[40,128]{1,0:T(8,128)S(1)} %get-tuple-element.78), channel_id=1, source_target_pairs={{0,4},{4,8},{8,12},{12,16},{16,20},{20,24},{24,28},{28,32},{32,36}... | collective-permute-start | bytes 61448 | tf_op jit(solution)/shard_map/ppermute | solution.py:744
  (43 other events, 219.4 us)
where the time goes:
time: 194 us; the launch traced here: 193 us
  waiting for transfers between devices  65 us (34%)
  starting transfers between devices  48.7 us (25%)
  blocking collectives  44.5 us (23%)
  Pallas kernels  20.5 us (11%)
  local copies, waits for them, and re-layouts  11.6 us (6%)
    all_to_all x1, blocking collectives, on_device(): returned = lax.all_to_all(summed, 'sp', 0, 0, tiled=True)  29.3 us
    pallas_call x14, Pallas kernels, kernel(): pl.pallas_call(body, out_shape=outs, in_specs=[smem] * len(lead) + [vmem]...  20.5 us
    all_to_all x1, waiting for transfers between devices, on_device(): got_grad = lax.all_to_all(sent_grad, 'sp', 0, 0, tiled=True)  16.5 us
    all_to_all x1, waiting for transfers between devices, on_device(): got_rows = lax.all_to_all(sent_rows, 'sp', 0, 0, tiled=True)  16.3 us
    all_to_all x1, blocking collectives, on_device(): token_grad = lax.all_to_all(token_copies, 'tp', 0, 0, tiled=True)  15.2 us
    all_to_all x1, starting transfers between devices, on_device(): got_rows = lax.all_to_all(sent_rows, 'sp', 0, 0, tiled=True)  13.1 us
    ppermute x1, waiting for transfers between devices, on_device(): got_left = lax.ppermute(to_right, 'tp', forward)  11.2 us
    unnamed x100, local copies, waits for them, and re-layouts  9.55 us
  transfers between devices with their start and end apart: 17, of which 8 were waited for; matrix products, arithmetic and copies ran while one was open for 2% of the time, Pallas kernels for 7%

commit v1 on v0

--- a/solution.py
+++ b/solution.py
@@ -21,15 +21,17 @@
     return forward, [(target, source) for source, target in forward]
 
 
-def ring_blocks(x, axis):
+def ring_blocks(top, bottom, axis):
     forward, backward = ring_pairs(axis)
-    half = x.shape[0] // 2
-    left = lax.ppermute(x, axis, forward)
-    right = lax.ppermute(x, axis, backward)
-    left_cut, right_cut = left[:half], right[half:]
-    far_top = lax.ppermute(left_cut, axis, forward)
-    far_bottom = lax.ppermute(right_cut, axis, backward)
-    return x, right, far_top, far_bottom, left
+    left_top = lax.ppermute(top, axis, forward)
+    right_bottom = lax.ppermute(bottom, axis, backward)
+    left_bottom = lax.ppermute(bottom, axis, forward)
+    right_top = lax.ppermute(top, axis, backward)
+    far_top = lax.ppermute(left_top, axis, forward)
+    far_bottom = lax.ppermute(right_bottom, axis, backward)
+    corner = left_top[:8, :LANES] + right_bottom[:8, :LANES]
+    near = (top, bottom, right_top, right_bottom, left_top, left_bottom)
+    return near, (far_top, far_bottom), corner
 
 
 def gelu_parts(values):
@@ -253,15 +255,26 @@
     out_ref[...] = scratch_ref[...].reshape(out_ref.shape).astype(jnp.bfloat16)
 
 
-def unpack_rows(in_ref, scratch_ref, out_ref, room):
+def unpack_rows(in_ref, scratch_ref, room, width):
     shards = in_ref.shape[0]
-    parts = out_ref.shape[1] // LANES
+    parts = width // LANES
     scratch_ref[...] = in_ref[...].astype(jnp.float32).reshape(scratch_ref.shape)
-    for r in range(room):
-        for c in range(parts):
-            out_ref[r * shards : (r + 1) * shards, c * LANES : (c + 1) * LANES] = scratch_ref[
-                pl.ds(row_of(r, c, parts), shards, stride=ROOM_PAD), :
-            ].astype(jnp.bfloat16)
+    return jnp.concatenate(
+        [
+            jnp.concatenate(
+                [
+                    scratch_ref[pl.ds(row_of(r, c, parts), shards, stride=ROOM_PAD), :]
+                    for c in range(parts)
+                ],
+                axis=1,
+            )
+            for r in range(room)
+        ]
+    ).astype(jnp.bfloat16)
+
+
+def joined(top_ref, bottom_ref):
+    return jnp.concatenate([top_ref[...], bottom_ref[...]])
 
 
 def first_dims(a, b):
@@ -327,8 +340,11 @@
     pack_rows(total, scratch_ref, packed_ref, slots // shards)
 
 
-def unpack_kernel(in_ref, out_ref, scratch_ref):
-    unpack_rows(in_ref, scratch_ref, out_ref, out_ref.shape[0] // in_ref.shape[0])
+def unpack_kernel(in_ref, top_ref, bottom_ref, scratch_ref):
+    half, width = top_ref.shape
+    rows = unpack_rows(in_ref, scratch_ref, 2 * half // in_ref.shape[0], width)
+    top_ref[...] = rows[:half]
+    bottom_ref[...] = rows[half:]
 
 
 def offsets(place_ref, groups, span):
@@ -337,31 +353,35 @@
     ]
 
 
+def pre_kernel(place_ref, *refs):
+    *blocks, gate_ref, up_ref, gate_out_ref, up_out_ref = refs
+    span = blocks[0].shape[1]
+    at = offsets(place_ref, gate_ref.shape[0] // span, span)
+    own, right, left = (joined(*blocks[k : k + 2]) for k in (0, 2, 4))
+    for w_ref, out_ref in ((gate_ref, gate_out_ref), (up_ref, up_out_ref)):
+        total = plain(own, w_ref[pl.ds(at[0], span), :])
+        total = total + plain(right, w_ref[pl.ds(at[1], span), :])
+        out_ref[...] = total + plain(left, w_ref[pl.ds(at[3], span), :])
+
+
 def forward_kernel(
     place_ref,
-    own_ref,
-    right_ref,
+    gate_near_ref,
+    up_near_ref,
     top_ref,
     bottom_ref,
-    left_ref,
     gate_ref,
     up_ref,
+    _corner_ref,
     act_ref,
     gate_factor_ref,
     up_factor_ref,
 ):
     _, span = top_ref.shape
     at = offsets(place_ref, gate_ref.shape[0] // span, span)
-    far = jnp.concatenate([top_ref[...], bottom_ref[...]])
-
-    def pre(w_ref):
-        total = plain(own_ref[...], w_ref[pl.ds(at[0], span), :])
-        total = total + plain(right_ref[...], w_ref[pl.ds(at[1], span), :])
-        total = total + plain(left_ref[...], w_ref[pl.ds(at[3], span), :])
-        return total + plain(far, w_ref[pl.ds(at[2], span), :])
-
-    gate_pre = pre(gate_ref)
-    up_pre = pre(up_ref)
+    far = joined(top_ref, bottom_ref)
+    gate_pre = gate_near_ref[...] + plain(far, gate_ref[pl.ds(at[2], span), :])
+    up_pre = up_near_ref[...] + plain(far, up_ref[pl.ds(at[2], span), :])
     gate = jnp.minimum(gate_pre, CLAMP_LIMIT)
     up_one = jnp.clip(up_pre, -CLAMP_LIMIT, CLAMP_LIMIT) + 1.0
     sig = jax.nn.sigmoid(SHARPNESS * gate)
@@ -373,12 +393,14 @@
     up_factor_ref[...] = jnp.where(jnp.abs(up_pre) < CLAMP_LIMIT, swish, 0.0)
 
 
-def near_kernel(place_ref, own_ref, right_ref, left_ref, down_ref, total_ref):
-    span = own_ref.shape[1]
+def near_kernel(place_ref, *refs):
+    *blocks, down_ref, total_ref = refs
+    span = blocks[0].shape[1]
     at = offsets(place_ref, down_ref.shape[1] // span, span)
-    total = last_dims(own_ref[...], down_ref[:, pl.ds(at[0], span)])
-    total = total + last_dims(right_ref[...], down_ref[:, pl.ds(at[1], span)])
-    total_ref[...] = total + last_dims(left_ref[...], down_ref[:, pl.ds(at[3], span)])
+    own, right, left = (joined(*blocks[k : k + 2]) for k in (0, 2, 4))
+    total = last_dims(own, down_ref[:, pl.ds(at[0], span)])
+    total = total + last_dims(right, down_ref[:, pl.ds(at[1], span)])
+    total_ref[...] = total + last_dims(left, down_ref[:, pl.ds(at[3], span)])
 
 
 def delta_kernel(
@@ -439,48 +461,26 @@
     pack_rows(total, scratch_ref, packed_ref, total.shape[0] // packed_ref.shape[0])
 
 
-def combine_kernel(in_ref, pick0_ref, pick1_ref, out_ref, scratch_ref, rows_ref):
-    unpack_rows(in_ref, scratch_ref, rows_ref, rows_ref.shape[0] // in_ref.shape[0])
-    total = first_dims(pick0_ref[...] + pick1_ref[...], rows_ref[...]).astype(jnp.bfloat16)
+def combine_kernel(in_ref, pick0_ref, pick1_ref, out_ref, scratch_ref):
+    pick = pick0_ref[...] + pick1_ref[...]
+    rows = unpack_rows(in_ref, scratch_ref, pick.shape[0] // in_ref.shape[0], out_ref.shape[2])
+    total = first_dims(pick, rows).astype(jnp.bfloat16)
     for k in range(out_ref.shape[0]):
         out_ref[k] = total
 
 
-def weights_kernel(
-    place_ref,
-    r_own_ref,
-    r_right_ref,
-    r_top_ref,
-    r_bottom_ref,
-    r_left_ref,
-    g_own_ref,
-    g_right_ref,
-    g_top_ref,
-    g_bottom_ref,
-    g_left_ref,
-    act_ref,
-    gate_delta_ref,
-    up_delta_ref,
-    gate_out_ref,
-    up_out_ref,
-    down_out_ref,
-):
-    _, span = r_top_ref.shape
+def weights_kernel(place_ref, *refs):
+    rows, grads = refs[:8], refs[8:16]
+    act_ref, gate_delta_ref, up_delta_ref, gate_out_ref, up_out_ref, down_out_ref = refs[16:]
+    span = rows[0].shape[1]
     at = offsets(place_ref, gate_out_ref.shape[0] // span, span)
-    rows = (r_own_ref, r_right_ref, (r_top_ref, r_bottom_ref), r_left_ref)
-    grads = (g_own_ref, g_right_ref, (g_top_ref, g_bottom_ref), g_left_ref)
     bf = jnp.bfloat16
-
-    def whole(block):
-        if isinstance(block, tuple):
-            return jnp.concatenate([part[...] for part in block])
-        return block[...]
-
-    for k in range(4):
-        row = whole(rows[k])
+    for k, first in ((0, 0), (1, 2), (3, 4), (2, 6)):
+        row = joined(*rows[first : first + 2])
+        grad = joined(*grads[first : first + 2])
         gate_out_ref[pl.ds(at[k], span), :] = first_dims(row, gate_delta_ref[...]).astype(bf)
         up_out_ref[pl.ds(at[k], span), :] = first_dims(row, up_delta_ref[...]).astype(bf)
-        down_out_ref[:, pl.ds(at[k], span)] = first_dims(act_ref[...], whole(grads[k])).astype(bf)
+        down_out_ref[:, pl.ds(at[k], span)] = first_dims(act_ref[...], grad).astype(bf)
 
 
 def on_device(
@@ -627,35 +627,41 @@
         )
     )
 
+    half = slot_count // 2
+
     def unpacked(x):
-        return kernel(unpack_kernel, shaped(slot_count, span), x, scratch=(pack_scratch,))
+        return kernel(
+            unpack_kernel, (shaped(half, span), shaped(half, span)), x, scratch=(pack_scratch,)
+        )
 
     got_rows = lax.all_to_all(sent_rows, "sp", 0, 0, tiled=True)
-    rows = ring_blocks(unpacked(got_rows), "tp")
+    rows, far_rows, corner = ring_blocks(*unpacked(got_rows), "tp")
     got_grad = lax.all_to_all(sent_grad, "sp", 0, 0, tiled=True)
-    grads = ring_blocks(unpacked(got_grad), "tp")
+    grads, far_grads, _ = ring_blocks(*unpacked(got_grad), "tp")
     wide_hidden = shaped(slot_count, hidden, dtype=f32)
-    act, gate_factor, up_factor = kernel(
-        forward_kernel,
-        (shaped(slot_count, hidden), wide_hidden, wide_hidden),
+    gate_near, up_near = kernel(
+        pre_kernel,
+        (wide_hidden, wide_hidden),
         *rows,
         gate_proj[0],
         up_proj[0],
         scalar=place,
-        flops=1 << 31,
-    )
-    half = slot_count // 2
-    forward, backward = ring_pairs("tp")
-    near = kernel(
-        near_kernel,
-        wide_hidden,
-        grads[0],
-        grads[1],
-        grads[4],
-        down_proj[0],
+        flops=1 << 30,
+    )
+    act, gate_factor, up_factor = kernel(
+        forward_kernel,
+        (shaped(slot_count, hidden), wide_hidden, wide_hidden),
+        gate_near,
+        up_near,
+        *far_rows,
+        gate_proj[0],
+        up_proj[0],
+        corner,
         scalar=place,
         flops=1 << 30,
     )
+    forward, backward = ring_pairs("tp")
+    near = kernel(near_kernel, wide_hidden, *grads, down_proj[0], scalar=place, flops=1 << 30)
     gate_delta, up_delta, far_top, far_bottom = kernel(
         delta_kernel,
         (
@@ -665,8 +671,7 @@
             shaped(half, span),
         ),
         near,
-        grads[2],
-        grads[3],
+        *far_grads,
         down_proj[0],
         gate_proj[0],
         up_proj[0],
@@ -707,7 +712,7 @@
         returned,
         pick0,
         pick1,
-        scratch=(pack_scratch, pltpu.VMEM((slot_count, span), bf16)),
+        scratch=(pack_scratch,),
     )
     token_grad = lax.all_to_all(token_copies, "tp", 0, 0, tiled=True)
     wide = shaped(2 * tok_rows, channels, dtype=f32)
@@ -750,7 +755,9 @@
             shaped(hidden, embedding_width),
         ),
         *rows,
+        *far_rows,
         *grads,
+        *far_grads,
         act,
         gate_delta,
         up_delta,

time: 194 us -> 205 us (1.057)
  blocking collectives: 44.5 us -> 78 us
  waiting for transfers between devices: 65 us -> 41.5 us
  starting transfers between devices: 48.7 us -> 40 us
  local copies, waits for them, and re-layouts: 11.6 us -> 19.3 us
    all_to_all x0 -> x1, blocking collectives: none -> 33.1 us  [on_device(): got_grad = lax.all_to_all(sent_grad, 'sp', 0, 0, tiled=True)]
    all_to_all x1 -> x0, waiting for transfers between devices: 16.5 us -> none  [on_device(): got_grad = lax.all_to_all(sent_grad, 'sp', 0, 0, tiled=True)]
    unnamed x100 -> x112, local copies, waits for them, and re-layouts: 9.55 us -> 17.6 us
    all_to_all x1, starting transfers between devices: 13.1 us -> 5.8 us  [on_device(): got_rows = lax.all_to_all(sent_rows, 'sp', 0, 0, tiled=True)]
    all_to_all x1 -> x0, starting transfers between devices: 5.8 us -> none  [on_device(): got_grad = lax.all_to_all(sent_grad, 'sp', 0, 0, tiled=True)]
    ppermute x8 -> x12, starting transfers between devices: 11.4 us -> 16.1 us  [the longest x2 6.33 us: ring_blocks(): far_bottom = lax.ppermute(right_bottom, axis, backward)]
    all_to_all x1, waiting for transfers between devices: 2.8 us -> 0.01 us  [on_device(): got = lax.all_to_all(sent, 'sp', 0, 0, tiled=True)]
    ppermute x8 -> x12, waiting for transfers between devices: 13.6 us -> 11.2 us  [the longest x2 9.4 us: ring_blocks(): far_top = lax.ppermute(left_top, axis, forward)]
  transfers between devices with their start and end apart: 17 -> 20, of which waited for: 8 -> 6; matrix products, arithmetic and copies ran while one was open for 2% -> 0% of each run, Pallas kernels for 7% -> 6%
where the time goes in v1:
time: 205 us; the launch traced here: 203 us
  blocking collectives  78 us (38%)
  waiting for transfers between devices  41.5 us (20%)
  starting transfers between devices  40 us (20%)
  local copies, waits for them, and re-layouts  19.3 us (9%)
  Pallas kernels  18.6 us (9%)
  other arithmetic  2.55 us (1%)
    all_to_all x1, blocking collectives, on_device(): got_grad = lax.all_to_all(sent_grad, 'sp', 0, 0, tiled=True)  33.1 us
    all_to_all x1, blocking collectives, on_device(): returned = lax.all_to_all(summed, 'sp', 0, 0, tiled=True)  29.7 us
    pallas_call x15, Pallas kernels, kernel(): pl.pallas_call(body, out_shape=outs, in_specs=[smem] * len(lead) + [vmem]...  18.6 us
    unnamed x112, local copies, waits for them, and re-layouts  17.6 us
    all_to_all x1, blocking collectives, on_device(): token_grad = lax.all_to_all(token_copies, 'tp', 0, 0, tiled=True)  15.2 us
    all_to_all x1, waiting for transfers between devices, on_device(): got_rows = lax.all_to_all(sent_rows, 'sp', 0, 0, tiled=True)  15.1 us
    ppermute x1, waiting for transfers between devices, on_device(): got_left = lax.ppermute(to_right, 'tp', forward)  10.9 us
    ppermute x2, waiting for transfers between devices, ring_blocks(): far_top = lax.ppermute(left_top, axis, forward)  9.4 us
  transfers between devices with their start and end apart: 20, of which 6 were waited for; matrix products, arithmetic and copies ran while one was open for 0% of the time, Pallas kernels for 6%

profile of v1, /device:TPU:1, one launch (start us, length us, event | category | flops | bytes accessed | tf_op | source)
XLA Modules:
  0.0 202.7 jit_solution(8564536824892218119)
XLA Ops:
  3.0 1.2 fusion.7
  9.8 33.1 %all_to_all.25.in_ref = bf16[64,40,128]{2,1,0:T(8,128)(2,1)S(1)} all-to-all(bf16[64,40,128]{2,1,0:T(8,128)(2,1)S(1)} %shard_map.201), channel_id=1, replica_groups=mesh['sp'=64,'tp'=4] {'sp'}, dimensions={0} | all-to-all | bytes 1310720 | tf_op jit(solution)/shard_map/all_to_all | solution.py:639
  42.9 5.8 %all-to-all-start = ((bf16[64,40,128]{2,1,0:T(8,128)(2,1)}), bf16[64,40,128]{2,1,0:T(8,128)(2,1)S(1)}, u32[]{:S(2)}, u32[]{:S(2)}) async-start(bf16[64,40,128]{2,1,0:T(8,128)(2,1)} %copy-done.11), calls=%async_computation | async-start | bytes 1310720 | tf_op jit(solution)/shard_map/all_to_all | solution.py:637
  49.8 2.7 %collective-permute-start.6 = (bf16[288,512]{1,0:T(8,128)(2,1)}, bf16[288,512]{1,0:T(8,128)(2,1)S(1)}, u32[]{:S(2)}, u32[]{:S(2)}) collective-permute-start(bf16[288,512]{1,0:T(8,128)(2,1)} %get-tuple-element.56.refs_0_.refs_8_), channel_id=1, source_target_pairs={{1,0},{2,1},{3,2},{0,3},{5,4},{6,5},{7,6},{4,7},{9,8},{10,9},{11,1... | collective-permute-start | bytes 884744 | tf_op jit(solution)/shard_map/ppermute | solution.py:29
  54.0 15.1 %all-to-all-done.in_ref = bf16[64,40,128]{2,1,0:T(8,128)(2,1)S(1)} async-done(((bf16[64,40,128]{2,1,0:T(8,128)(2,1)}), bf16[64,40,128]{2,1,0:T(8,128)(2,1)S(1)}, u32[]{:S(2)}, u32[]{:S(2)}) %all-to-all-start) | async-done | bytes 655392 | tf_op jit(solution)/shard_map/all_to_all | solution.py:637
  69.4 2.8 %collective-permute-start = (bf16[288,512]{1,0:T(8,128)(2,1)S(1)}, bf16[288,512]{1,0:T(8,128)(2,1)S(1)}, u32[]{:S(2)}, u32[]{:S(2)}) collective-permute-start(bf16[288,512]{1,0:T(8,128)(2,1)S(1)} %get-tuple-element.51.refs_0_), channel_id=1, source_target_pairs={{1,0},{2,1},{3,2},{0,3},{5,4},{6,5},{7,6},{4,7},{9,8},{10,9},{11,1... | collective-permute-start | bytes 884744 | tf_op jit(solution)/shard_map/ppermute | solution.py:29
  72.9 2.7 %collective-permute-start.1 = (bf16[288,512]{1,0:T(8,128)(2,1)S(1)}, bf16[288,512]{1,0:T(8,128)(2,1)S(1)}, u32[]{:S(2)}, u32[]{:S(2)}) collective-permute-start(bf16[288,512]{1,0:T(8,128)(2,1)S(1)} %get-tuple-element.52.refs_1_), channel_id=1, source_target_pairs={{1,0},{2,1},{3,2},{0,3},{5,4},{6,5},{7,6},{4,7},{9,8},{10,9},{11,1... | collective-permute-start | bytes 884744 | tf_op jit(solution)/shard_map/ppermute | solution.py:27
  75.7 1.2 copy-done.2
  77.9 2.1 %shard_map.205.near_ref = f32[576,256]{1,0:T(8,128)S(1)} custom-call(s32[1]{0:T(128)} %bitcast.place_ref, bf16[288,512]{1,0:T(8,128)(2,1)} %get-tuple-element.56.refs_0_.refs_8_, bf16[288,512]{1,0:T(8,128)(2,1)} %get-tuple-element.57.refs_1_.refs_9_, bf16[288,512]{1,0:T(8,128)(2,1)S(1)} %copy-done.23, ...), custom_call_target="tpu_custom_call" | custom-call | flops 1073741824 | tf_op jit(solution)/shard_map/pallas_call | solution.py:524
  80.1 2.9 %collective-permute-start.11 = (bf16[288,512]{1,0:T(8,128)(2,1)}, bf16[288,512]{1,0:T(8,128)(2,1)S(1)}, u32[]{:S(2)}, u32[]{:S(2)}) collective-permute-start(bf16[288,512]{1,0:T(8,128)(2,1)} %collective-permute-done.7.refs_3_.refs_11_), channel_id=1, source_target_pairs={{1,0},{2,1},{3,2},{0,3},{5,4},{6,5},{7,6},{4,7},{9,8},{10,9},{11,1... | collective-permute-start | bytes 884744 | tf_op jit(solution)/shard_map/ppermute | solution.py:31
  83.0 1.3 collective-permute-done.1.refs_3_
  84.3 3.4 %collective-permute-start.5 = (bf16[288,512]{1,0:T(8,128)(2,1)S(1)}, bf16[288,512]{1,0:T(8,128)(2,1)S(1)}, u32[]{:S(2)}, u32[]{:S(2)}) collective-permute-start(bf16[288,512]{1,0:T(8,128)(2,1)S(1)} %collective-permute-done.1.refs_3_), channel_id=1, source_target_pairs={{1,0},{2,1},{3,2},{0,3},{5,4},{6,5},{7,6},{4,7},{9,8},{10,9},{11,1... | collective-permute-start | bytes 884744 | tf_op jit(solution)/shard_map/ppermute | solution.py:31
  91.4 9.4 %collective-permute-done.4.top_ref.refs_6_ = bf16[288,512]{1,0:T(8,128)(2,1)S(1)} collective-permute-done((bf16[288,512]{1,0:T(8,128)(2,1)S(1)}, bf16[288,512]{1,0:T(8,128)(2,1)S(1)}, u32[]{:S(2)}, u32[]{:S(2)}) %collective-permute-start.4) | collective-permute-done | bytes 294944 | tf_op jit(solution)/shard_map/ppermute | solution.py:30
  103.3 2.7 %collective-permute-start.13 = (bf16[288,512]{1,0:T(8,128)(2,1)S(1)}, bf16[288,512]{1,0:T(8,128)(2,1)S(1)}, u32[]{:S(2)}, u32[]{:S(2)}) collective-permute-start(bf16[288,512]{1,0:T(8,128)(2,1)S(1)} %get-tuple-element.72), channel_id=1, source_target_pairs={{1,0},{2,1},{3,2},{0,3},{5,4},{6,5},{7,6},{4,7},{9,8},{10,9},{11,1... | collective-permute-start | bytes 884744 | tf_op jit(solution)/shard_map/ppermute | solution.py:683
  107.1 4.3 %collective-permute-done.12.from_left_ref = bf16[288,512]{1,0:T(8,128)(2,1)S(1)} collective-permute-done((bf16[288,512]{1,0:T(8,128)(2,1)S(1)}, bf16[288,512]{1,0:T(8,128)(2,1)S(1)}, u32[]{:S(2)}, u32[]{:S(2)}) %collective-permute-start.12) | collective-permute-done | bytes 294944 | tf_op jit(solution)/shard_map/ppermute | solution.py:682
  111.7 2.7 %collective-permute-start.15 = (bf16[576,512]{1,0:T(8,128)(2,1)S(1)}, bf16[576,512]{1,0:T(8,128)(2,1)S(1)}, u32[]{:S(2)}, u32[]{:S(2)}) collective-permute-start(bf16[576,512]{1,0:T(8,128)(2,1)S(1)} %get-tuple-element.74), channel_id=1, source_target_pairs={{1,0},{2,1},{3,2},{0,3},{5,4},{6,5},{7,6},{4,7},{9,8},{10,9},{11,1... | collective-permute-start | bytes 1769480 | tf_op jit(solution)/shard_map/ppermute | solution.py:704
  114.4 10.9 %collective-permute-done.14.from_left_ref = bf16[576,512]{1,0:T(8,128)(2,1)S(1)} collective-permute-done((bf16[576,512]{1,0:T(8,128)(2,1)S(1)}, bf16[576,512]{1,0:T(8,128)(2,1)S(1)}, u32[]{:S(2)}, u32[]{:S(2)}) %collective-permute-start.14) | collective-permute-done | bytes 589856 | tf_op jit(solution)/shard_map/ppermute | solution.py:703
  125.7 29.7 %all_to_all.26.in_ref = bf16[64,40,128]{2,1,0:T(8,128)(2,1)S(1)} all-to-all(bf16[64,40,128]{2,1,0:T(8,128)(2,1)S(1)} %shard_map.210), channel_id=1, replica_groups=mesh['sp'=64,'tp'=4] {'sp'}, dimensions={0} | all-to-all | bytes 1310720 | tf_op jit(solution)/shard_map/all_to_all | solution.py:708
  155.9 15.2 %all_to_all.27.token_ref = bf16[4,192,512]{2,1,0:T(8,128)(2,1)S(1)} all-to-all(bf16[4,192,512]{2,1,0:T(8,128)(2,1)S(1)} %shard_map.211), channel_id=1, replica_groups=mesh['sp'=64,'tp'=4] {'tp'}, dimensions={0} | all-to-all | bytes 1572864 | tf_op jit(solution)/shard_map/all_to_all | solution.py:717
  171.2 2.3 %shard_map.212 = (bf16[192,128]{1,0:T(8,128)(2,1)}, f32[384,128]{1,0:T(8,128)S(1)}, f32[384,128]{1,0:T(8,128)S(1)}, bf16[64,40,128]{2,1,0:T(8,128)(2,1)}, f32[40,128]{1,0:T(8,128)S(1)}, /*index=5*/f32[40,128]{1,0:T(8,128)S(1)}) custom-call(bf16[4,192,512]{2,1,0:T(8,128)(2,1)S(1)} %all_to_all.27.token_ref, bf16[192,2048]{1,0:T(8,128)(2,1)S(1)} %copy-done, ...), custom_call_target="tpu_custom_call" | custom-call | tf_op jit(solution)/shard_map/pallas_call | solution.py:524
  173.5 7.1 %all-to-all-start.4 = ((bf16[64,40,128]{2,1,0:T(8,128)(2,1)}), bf16[64,40,128]{2,1,0:T(8,128)(2,1)S(1)}, u32[]{:S(2)}, u32[]{:S(2)}) async-start(bf16[64,40,128]{2,1,0:T(8,128)(2,1)} %get-tuple-element.83), calls=%async_computation.4 | async-start | bytes 1310720 | tf_op jit(solution)/shard_map/all_to_all | solution.py:747
  180.7 2.4 %collective-permute-start.16 = (f32[40,128]{1,0:T(8,128)S(1)}, f32[40,128]{1,0:T(8,128)S(1)}, u32[]{:S(2)}, u32[]{:S(2)}) collective-permute-start(f32[40,128]{1,0:T(8,128)S(1)} %get-tuple-element.89), channel_id=1, source_target_pairs={{4,0},{8,4},{12,8},{16,12},{20,16},{24,20},{28,24},{32,28},{36,32}... | collective-permute-start | bytes 61448 | tf_op jit(solution)/shard_map/ppermute | solution.py:748
  183.1 3.2 %collective-permute-start.17 = (f32[40,128]{1,0:T(8,128)S(1)}, f32[40,128]{1,0:T(8,128)S(1)}, u32[]{:S(2)}, u32[]{:S(2)}) collective-permute-start(f32[40,128]{1,0:T(8,128)S(1)} %get-tuple-element.90), channel_id=1, source_target_pairs={{0,4},{4,8},{8,12},{12,16},{16,20},{20,24},{24,28},{28,32},{32,36}... | collective-permute-start | bytes 61448 | tf_op jit(solution)/shard_map/ppermute | solution.py:749
  195.9 5.5 %shard_map.207 = (bf16[2048,256]{1,0:T(8,128)(2,1)}, bf16[2048,256]{1,0:T(8,128)(2,1)}, bf16[256,2048]{1,0:T(8,128)(2,1)}) custom-call(s32[1]{0:T(128)} %bitcast.place_ref, bf16[288,512]{1,0:T(8,128)(2,1)S(1)} %copy-done.26, bf16[288,512]{1,0:T(8,128)(2,1)S(1)} %copy-done.28, bf16[288,512]{1,0:T(8,128)(2,1)S(1)} %copy-done.30, ...), custom_call_target="tpu_custom_call" | custom-call | flops 2147483648 | tf_op jit(solution)/shard_map/pallas_call | solution.py:524
  (160 shorter events, 31.8 us)
Async XLA Ops:
  42.9 26.2 %all-to-all-start = ((bf16[64,40,128]{2,1,0:T(8,128)(2,1)}), bf16[64,40,128]{2,1,0:T(8,128)(2,1)S(1)}, u32[]{:S(2)}, u32[]{:S(2)}) async-start(bf16[64,40,128]{2,1,0:T(8,128)(2,1)} %copy-done.11), calls=%async_computation | async-start | bytes 1310720 | tf_op jit(solution)/shard_map/all_to_all | solution.py:637
  49.8 22.4 %collective-permute-start.6 = (bf16[288,512]{1,0:T(8,128)(2,1)}, bf16[288,512]{1,0:T(8,128)(2,1)S(1)}, u32[]{:S(2)}, u32[]{:S(2)}) collective-permute-start(bf16[288,512]{1,0:T(8,128)(2,1)} %get-tuple-element.56.refs_0_.refs_8_), channel_id=1, source_target_pairs={{1,0},{2,1},{3,2},{0,3},{5,4},{6,5},{7,6},{4,7},{9,8},{10,9},{11,1... | collective-permute-start | bytes 884744 | tf_op jit(solution)/shard_map/ppermute | solution.py:29
  52.5 20.4 %collective-permute-start.7 = (bf16[288,512]{1,0:T(8,128)(2,1)}, bf16[288,512]{1,0:T(8,128)(2,1)}, u32[]{:S(2)}, u32[]{:S(2)}) collective-permute-start(bf16[288,512]{1,0:T(8,128)(2,1)} %get-tuple-element.57.refs_1_.refs_9_), channel_id=1, source_target_pairs={{1,0},{2,1},{3,2},{0,3},{5,4},{6,5},{7,6},{4,7},{9,8},{10,9},{11,1... | collective-permute-start | bytes 884744 | tf_op jit(solution)/shard_map/ppermute | solution.py:27
  53.0 22.6 %collective-permute-start.8 = (bf16[288,512]{1,0:T(8,128)(2,1)}, bf16[288,512]{1,0:T(8,128)(2,1)}, u32[]{:S(2)}, u32[]{:S(2)}) collective-permute-start(bf16[288,512]{1,0:T(8,128)(2,1)} %get-tuple-element.56.refs_0_.refs_8_), channel_id=1, source_target_pairs={{0,1},{1,2},{2,3},{3,0},{4,5},{5,6},{6,7},{7,4},{8,9},{9,10},{10,1... | collective-permute-start | bytes 884744 | tf_op jit(solution)/shard_map/ppermute | solution.py:26
  54.0 21.6 %collective-permute-start.9 = (bf16[288,512]{1,0:T(8,128)(2,1)}, bf16[288,512]{1,0:T(8,128)(2,1)}, u32[]{:S(2)}, u32[]{:S(2)}) collective-permute-start(bf16[288,512]{1,0:T(8,128)(2,1)} %get-tuple-element.57.refs_1_.refs_9_), channel_id=1, source_target_pairs={{0,1},{1,2},{2,3},{3,0},{4,5},{5,6},{6,7},{7,4},{8,9},{9,10},{10,1... | collective-permute-start | bytes 884744 | tf_op jit(solution)/shard_map/ppermute | solution.py:28
  69.4 10.7 %collective-permute-start = (bf16[288,512]{1,0:T(8,128)(2,1)S(1)}, bf16[288,512]{1,0:T(8,128)(2,1)S(1)}, u32[]{:S(2)}, u32[]{:S(2)}) collective-permute-start(bf16[288,512]{1,0:T(8,128)(2,1)S(1)} %get-tuple-element.51.refs_0_), channel_id=1, source_target_pairs={{1,0},{2,1},{3,2},{0,3},{5,4},{6,5},{7,6},{4,7},{9,8},{10,9},{11,1... | collective-permute-start | bytes 884744 | tf_op jit(solution)/shard_map/ppermute | solution.py:29
  72.9 10.1 %collective-permute-start.2 = (bf16[288,512]{1,0:T(8,128)(2,1)S(1)}, bf16[288,512]{1,0:T(8,128)(2,1)S(1)}, u32[]{:S(2)}, u32[]{:S(2)}) collective-permute-start(bf16[288,512]{1,0:T(8,128)(2,1)S(1)} %get-tuple-element.51.refs_0_), channel_id=1, source_target_pairs={{0,1},{1,2},{2,3},{3,0},{4,5},{5,6},{6,7},{7,4},{8,9},{9,10},{10,1... | collective-permute-start | bytes 884744 | tf_op jit(solution)/shard_map/ppermute | solution.py:26
  72.9 11.4 %collective-permute-start.1 = (bf16[288,512]{1,0:T(8,128)(2,1)S(1)}, bf16[288,512]{1,0:T(8,128)(2,1)S(1)}, u32[]{:S(2)}, u32[]{:S(2)}) collective-permute-start(bf16[288,512]{1,0:T(8,128)(2,1)S(1)} %get-tuple-element.52.refs_1_), channel_id=1, source_target_pairs={{1,0},{2,1},{3,2},{0,3},{5,4},{6,5},{7,6},{4,7},{9,8},{10,9},{11,1... | collective-permute-start | bytes 884744 | tf_op jit(solution)/shard_map/ppermute | solution.py:27
  75.6 12.6 %collective-permute-start.3 = (bf16[288,512]{1,0:T(8,128)(2,1)S(1)}, bf16[288,512]{1,0:T(8,128)(2,1)S(1)}, u32[]{:S(2)}, u32[]{:S(2)}) collective-permute-start(bf16[288,512]{1,0:T(8,128)(2,1)S(1)} %get-tuple-element.52.refs_1_), channel_id=1, source_target_pairs={{0,1},{1,2},{2,3},{3,0},{4,5},{5,6},{6,7},{7,4},{8,9},{9,10},{10,1... | collective-permute-start | bytes 884744 | tf_op jit(solution)/shard_map/ppermute | solution.py:28
  75.6 26.0 %collective-permute-start.10 = (bf16[288,512]{1,0:T(8,128)(2,1)}, bf16[288,512]{1,0:T(8,128)(2,1)S(1)}, u32[]{:S(2)}, u32[]{:S(2)}) collective-permute-start(bf16[288,512]{1,0:T(8,128)(2,1)} %collective-permute-done.8.refs_4_.refs_12_), channel_id=1, source_target_pairs={{0,1},{1,2},{2,3},{3,0},{4,5},{5,6},{6,7},{7,4},{8,9},{9,10},{10,1... | collective-permute-start | bytes 884744 | tf_op jit(solution)/shard_map/ppermute | solution.py:30
  80.1 21.6 %collective-permute-start.11 = (bf16[288,512]{1,0:T(8,128)(2,1)}, bf16[288,512]{1,0:T(8,128)(2,1)S(1)}, u32[]{:S(2)}, u32[]{:S(2)}) collective-permute-start(bf16[288,512]{1,0:T(8,128)(2,1)} %collective-permute-done.7.refs_3_.refs_11_), channel_id=1, source_target_pairs={{1,0},{2,1},{3,2},{0,3},{5,4},{6,5},{7,6},{4,7},{9,8},{10,9},{11,1... | collective-permute-start | bytes 884744 | tf_op jit(solution)/shard_map/ppermute | solution.py:31
  83.0 17.9 %collective-permute-start.4 = (bf16[288,512]{1,0:T(8,128)(2,1)S(1)}, bf16[288,512]{1,0:T(8,128)(2,1)S(1)}, u32[]{:S(2)}, u32[]{:S(2)}) collective-permute-start(bf16[288,512]{1,0:T(8,128)(2,1)S(1)} %collective-permute-done.2.refs_4_), channel_id=1, source_target_pairs={{0,1},{1,2},{2,3},{3,0},{4,5},{5,6},{6,7},{7,4},{8,9},{9,10},{10,1... | collective-permute-start | bytes 884744 | tf_op jit(solution)/shard_map/ppermute | solution.py:30
  84.3 16.5 %collective-permute-start.5 = (bf16[288,512]{1,0:T(8,128)(2,1)S(1)}, bf16[288,512]{1,0:T(8,128)(2,1)S(1)}, u32[]{:S(2)}, u32[]{:S(2)}) collective-permute-start(bf16[288,512]{1,0:T(8,128)(2,1)S(1)} %collective-permute-done.1.refs_3_), channel_id=1, source_target_pairs={{1,0},{2,1},{3,2},{0,3},{5,4},{6,5},{7,6},{4,7},{9,8},{10,9},{11,1... | collective-permute-start | bytes 884744 | tf_op jit(solution)/shard_map/ppermute | solution.py:31
  103.3 8.2 %collective-permute-start.12 = (bf16[288,512]{1,0:T(8,128)(2,1)S(1)}, bf16[288,512]{1,0:T(8,128)(2,1)S(1)}, u32[]{:S(2)}, u32[]{:S(2)}) collective-permute-start(bf16[288,512]{1,0:T(8,128)(2,1)S(1)} %get-tuple-element.71), channel_id=1, source_target_pairs={{0,1},{1,2},{2,3},{3,0},{4,5},{5,6},{6,7},{7,4},{8,9},{9,10},{10,1... | collective-permute-start | bytes 884744 | tf_op jit(solution)/shard_map/ppermute | solution.py:682
  103.3 8.1 %collective-permute-start.13 = (bf16[288,512]{1,0:T(8,128)(2,1)S(1)}, bf16[288,512]{1,0:T(8,128)(2,1)S(1)}, u32[]{:S(2)}, u32[]{:S(2)}) collective-permute-start(bf16[288,512]{1,0:T(8,128)(2,1)S(1)} %get-tuple-element.72), channel_id=1, source_target_pairs={{1,0},{2,1},{3,2},{0,3},{5,4},{6,5},{7,6},{4,7},{9,8},{10,9},{11,1... | collective-permute-start | bytes 884744 | tf_op jit(solution)/shard_map/ppermute | solution.py:683
  111.6 13.6 %collective-permute-start.14 = (bf16[576,512]{1,0:T(8,128)(2,1)S(1)}, bf16[576,512]{1,0:T(8,128)(2,1)S(1)}, u32[]{:S(2)}, u32[]{:S(2)}) collective-permute-start(bf16[576,512]{1,0:T(8,128)(2,1)S(1)} %get-tuple-element.73), channel_id=1, source_target_pairs={{0,1},{1,2},{2,3},{3,0},{4,5},{5,6},{6,7},{7,4},{8,9},{9,10},{10,1... | collective-permute-start | bytes 1769480 | tf_op jit(solution)/shard_map/ppermute | solution.py:703
  111.7 13.5 %collective-permute-start.15 = (bf16[576,512]{1,0:T(8,128)(2,1)S(1)}, bf16[576,512]{1,0:T(8,128)(2,1)S(1)}, u32[]{:S(2)}, u32[]{:S(2)}) collective-permute-start(bf16[576,512]{1,0:T(8,128)(2,1)S(1)} %get-tuple-element.74), channel_id=1, source_target_pairs={{1,0},{2,1},{3,2},{0,3},{5,4},{6,5},{7,6},{4,7},{9,8},{10,9},{11,1... | collective-permute-start | bytes 1769480 | tf_op jit(solution)/shard_map/ppermute | solution.py:704
  155.9 15.3 %copy-start.10 = (f32[2,192,128]{2,1,0:T(8,128)S(1)}, f32[2,192,128]{2,1,0:T(8,128)}, u32[]{:S(2)}) copy-start(f32[2,192,128]{2,1,0:T(8,128)} %get-tuple-element.79) | copy-start | bytes 589828
  155.9 15.3 %copy-start.12 = (bf16[128,2048]{1,0:T(8,128)(2,1)S(1)}, bf16[128,2048]{1,0:T(8,128)(2,1)}, u32[]{:S(2)}) copy-start(bf16[128,2048]{1,0:T(8,128)(2,1)} %out_proj_ref.1) | copy-start | bytes 1572868
  155.9 15.2 %copy-start.13 = (f32[192,128]{1,0:T(8,128)S(1)}, f32[192,128]{1,0:T(8,128)}, u32[]{:S(2)}) copy-start(f32[192,128]{1,0:T(8,128)} %get-tuple-element.76.states_ref) | copy-start | bytes 294916
  155.9 15.2 %copy-start.14 = (f32[192,128]{1,0:T(8,128)S(1)}, f32[192,128]{1,0:T(8,128)}, u32[]{:S(2)}) copy-start(f32[192,128]{1,0:T(8,128)} %get-tuple-element.78.slope_ref) | copy-start | bytes 294916
  173.5 27.9 %all-to-all-start.4 = ((bf16[64,40,128]{2,1,0:T(8,128)(2,1)}), bf16[64,40,128]{2,1,0:T(8,128)(2,1)S(1)}, u32[]{:S(2)}, u32[]{:S(2)}) async-start(bf16[64,40,128]{2,1,0:T(8,128)(2,1)} %get-tuple-element.83), calls=%async_computation.4 | async-start | bytes 1310720 | tf_op jit(solution)/shard_map/all_to_all | solution.py:747
  180.7 20.7 %collective-permute-start.16 = (f32[40,128]{1,0:T(8,128)S(1)}, f32[40,128]{1,0:T(8,128)S(1)}, u32[]{:S(2)}, u32[]{:S(2)}) collective-permute-start(f32[40,128]{1,0:T(8,128)S(1)} %get-tuple-element.89), channel_id=1, source_target_pairs={{4,0},{8,4},{12,8},{16,12},{20,16},{24,20},{28,24},{32,28},{36,32}... | collective-permute-start | bytes 61448 | tf_op jit(solution)/shard_map/ppermute | solution.py:748
  183.1 18.3 %collective-permute-start.17 = (f32[40,128]{1,0:T(8,128)S(1)}, f32[40,128]{1,0:T(8,128)S(1)}, u32[]{:S(2)}, u32[]{:S(2)}) collective-permute-start(f32[40,128]{1,0:T(8,128)S(1)} %get-tuple-element.90), channel_id=1, source_target_pairs={{0,4},{4,8},{8,12},{12,16},{16,20},{20,24},{24,28},{28,32},{32,36}... | collective-permute-start | bytes 61448 | tf_op jit(solution)/shard_map/ppermute | solution.py:749
  (52 other events, 176.4 us)
